TPU v7x, 32 devices: a whole 2x2x4 slice. The times are simulated.
32 devices in a mesh: ep: 8 (over z, y), tp: 4 (over x, core).
Axes of the slice: x: 2, y: 2, z: 4, core: 2. Of those that a mesh axis runs over, the one named last changes fastest.
Arguments:
- tokens: bfloat16 [1024, 2048], P('ep'), may hold values from -6 to 6
- norm_gain: float32 [2048], replicated, may hold values from 0.1 to 1.9
- expert_ids: int32 [1024, 6], P('ep'), may hold values from 0 to 15, all different within a row; in each aligned block of 128 rows (0 to 127, 128 to 255, ...) at most 96 rows name the same one
- route_weights: float32 [1024, 6], P('ep'), may hold values from 0.1 to 1
- expert_gate: bfloat16 [32, 2048, 256], P(('ep', 'tp')), may hold values from -0.125 to 0.125
- expert_up: bfloat16 [32, 2048, 256], P(('ep', 'tp')), may hold values from -0.125 to 0.125
- expert_down: bfloat16 [32, 256, 2048], P(('ep', 'tp')), may hold values from -0.25 to 0.25
- shared_gate: bfloat16 [2048, 512], P(None, 'tp'), may hold values from -0.125 to 0.125
- shared_up: bfloat16 [2048, 512], P(None, 'tp'), may hold values from -0.125 to 0.125
- shared_down: bfloat16 [512, 2048], P(None, 'tp'), may hold values from -0.25 to 0.25
Outputs:
- mixed: bfloat16 [1024, 2048], P('ep', 'tp')
Inputs may be any that keep to these rules, and one draw needn't show every extreme that they name: `expert_ids`: each row names 6 different experts. In each aligned block of 128 rows (the rows of one index of ep) no expert is named by more than 96 rows, a bound that some block reaches.
All inputs are finite; a program needn't handle non-finite values.
Results may differ from a plain program's by a relative error of at most 0.0073.
Values may be sent and summed in bfloat16 or wider, within the bound.
A program may use at most 64 MiB of HBM per device.

v0:
```python
import functools

import jax
import jax.numpy as jnp
from jax import lax
from jax.experimental import pallas as pl
from jax.experimental.pallas import tpu as pltpu
from jax.sharding import PartitionSpec as P

NORM_EPSILON = 1e-06


def swapped(block, axis, distance):
    count = lax.axis_size(axis)
    route = []
    for low in range(count):
        high = low | 1 << distance
        if high != low and high < count:
            route += [(low, high), (high, low)]
    return lax.ppermute(block, axis, route)


def routed_exchange(
    tokens,
    norm_gain,
    expert_ids,
    route_weights,
    expert_gate,
    expert_up,
    expert_down,
    shared_gate,
    shared_up,
    shared_down,
):
    ep_count = lax.axis_size("ep")
    tp_count = lax.axis_size("tp")
    pair_count = tp_count // 2
    tp_index = lax.axis_index("tp")
    column = tp_index // 2
    half_index = tp_index % 2
    token_count, model_width = tokens.shape
    top_count = expert_ids.shape[1]
    expert_count = ep_count * pair_count
    capacity = 2 * max(1, token_count * top_count // expert_count)
    half_cap = capacity // 2
    as_float = tokens.astype(jnp.float32)
    inverse_rms = lax.rsqrt(jnp.mean(as_float * as_float, axis=-1, keepdims=True) + NORM_EPSILON)
    normed = (as_float * inverse_rms * norm_gain).astype(jnp.bfloat16)
    expert_iota = jnp.arange(expert_count, dtype=jnp.int32)
    token_iota = jnp.arange(token_count, dtype=jnp.int32)
    counts = jnp.sum(
        (expert_ids[:, :, None] == expert_iota[None, None, :]).astype(jnp.bfloat16), axis=1
    )
    strict_lower = (token_iota[:, None] > token_iota[None, :]).astype(jnp.bfloat16)
    prefix = jnp.dot(strict_lower, counts, preferred_element_type=jnp.float32)
    slot_index = jnp.take_along_axis(prefix, expert_ids, axis=1).astype(jnp.int32)
    target = expert_ids // pair_count
    owner_column = expert_ids % pair_count
    is_mine = owner_column == column
    position = target * capacity + slot_index
    slot_iota = jnp.arange(ep_count * capacity, dtype=jnp.int32)
    matches = is_mine[None, :, :] & (position[None, :, :] == slot_iota[:, None, None])
    slot_taken = jnp.any(matches, axis=2)
    token_of_slot = jnp.sum(jnp.where(slot_taken, token_iota[None, :], 0), axis=1)
    filled = jnp.any(slot_taken, axis=1)
    buffer = jnp.where(
        filled[:, None], jnp.take(normed, token_of_slot, axis=0), jnp.zeros((), jnp.bfloat16)
    )
    buffer = buffer.reshape(ep_count, capacity, model_width)
    gate_local = expert_gate[0]
    up_local = expert_up[0]
    down_local = expert_down[0]
    received = lax.all_to_all(buffer, "ep", split_axis=0, concat_axis=0, tiled=True)
    flat_rows = received.reshape(-1, model_width)
    hidden = (
        jax.nn.silu(jnp.dot(flat_rows, gate_local, preferred_element_type=jnp.float32))
        * jnp.dot(flat_rows, up_local, preferred_element_type=jnp.float32)
    ).astype(jnp.bfloat16)
    partial_out = jnp.dot(hidden, down_local, preferred_element_type=jnp.float32).astype(
        jnp.bfloat16
    )
    partial_out = partial_out.reshape(received.shape[0], received.shape[1], model_width)
    kept_part = lax.dynamic_slice_in_dim(partial_out, half_index * half_cap, half_cap, 1)
    other_part = lax.dynamic_slice_in_dim(partial_out, (1 - half_index) * half_cap, half_cap, 1)
    partner_part = swapped(other_part, "tp", 0)
    expert_out = (kept_part.astype(jnp.float32) + partner_part.astype(jnp.float32)).astype(
        jnp.bfloat16
    )
    returned = lax.all_to_all(expert_out, "ep", split_axis=0, concat_axis=0, tiled=True)
    row_total = ep_count * half_cap
    flat_rows = returned.reshape(row_total, model_width).astype(jnp.float32)
    is_valid = is_mine & (slot_index // half_cap == half_index)
    row_index = jnp.where(is_valid, target * half_cap + slot_index % half_cap, -1)
    row_iota = jnp.arange(row_total, dtype=jnp.int32)
    hits = row_index[:, :, None] == row_iota[None, None, :]
    combine_table = jnp.sum(jnp.where(hits, route_weights[:, :, None], 0.0), axis=1)
    partial_routed = jnp.dot(
        combine_table,
        flat_rows,
        precision=lax.Precision.HIGHEST,
        preferred_element_type=jnp.float32,
    )
    routed = lax.psum_scatter(partial_routed, "tp", scatter_dimension=1, tiled=True)
    shared_act = (
        jax.nn.silu(jnp.dot(normed, shared_gate, preferred_element_type=jnp.float32))
        * jnp.dot(normed, shared_up, preferred_element_type=jnp.float32)
    ).astype(jnp.bfloat16)
    shared_out = jnp.dot(
        lax.all_gather(shared_act, "tp", axis=1, tiled=True),
        shared_down,
        preferred_element_type=jnp.float32,
    )
    return (routed + shared_out).astype(jnp.bfloat16)


MESH = pl.DeviceIdType.MESH
LANES = 128


def silu(v):
    return v / (1.0 + jnp.exp(-v))


def dense_kernel(
    ep_count, tp_count, minor, split,
    tok_ref, gain_ref, wt_ref, gate_hbm, up_hbm, down_hbm, sg_hbm, su_hbm, sd_hbm,
    out_ref,
    x_buf, y_buf, c_buf, xs_buf, xr_buf, ysa_buf, yra_buf, zsa_buf, zra_buf, zs_buf, zr_buf,
    ys_buf, yr_buf, fs_buf, fr_buf,
    acc, wt_all, sh_all, sh_out, gate, up, down, sg, su, sd,
    load_sem, wt_s, wt_r, sh_s, sh_r, y_s, u_s, d_s, z_r, x_s, x_r, c_s, c_r,
    ya_s, ya_r, yc_s, yc_r, rx_s, rx_r, rya_s, rya_r, rza_s, rza_r, rz_s, rz_r, ry_s, ry_r,
    f_s, f_r,
):
    major = ep_count // minor
    rows = tok_ref.shape[0]
    quarter = x_buf.shape[3]
    e = lax.axis_index("ep")
    t = lax.axis_index("tp")
    z = e // minor
    y = e % minor
    xi = t // 2
    c = t % 2
    t2 = 2 * (1 - xi) + c
    mate_x = {"tp": t2}
    mate_c = {"tp": 2 * xi + 1 - c}
    mate_y = {"ep": z * minor + 1 - y}
    z_up = {"ep": lax.rem(e + minor, ep_count)}
    z_down = {"ep": lax.rem(e + ep_count - minor, ep_count)}
    head_cols = pl.ds(0, split)
    rest_cols = pl.ds(split, quarter - split)

    def remote(src, dst, s, r, who):
        return pltpu.make_async_remote_copy(
            src_ref=src, dst_ref=dst, send_sem=s, recv_sem=r, device_id=who, device_id_type=MESH
        )

    loads = [
        pltpu.make_async_copy(a, b, load_sem.at[i])
        for i, (a, b) in enumerate(
            ((sg_hbm, sg), (su_hbm, su), (gate_hbm, gate), (up_hbm, up), (down_hbm, down), (sd_hbm, sd))
        )
    ]
    for load in loads:
        load.start()

    barrier = pltpu.get_barrier_semaphore()
    for k in range(1, ep_count):
        pl.semaphore_signal(barrier, inc=1, device_id={"ep": lax.rem(e + k, ep_count)}, device_id_type=MESH)
    for k in range(1, tp_count):
        pl.semaphore_signal(barrier, inc=1, device_id={"tp": lax.rem(t + k, tp_count)}, device_id_type=MESH)

    step = 16

    def norm_rows(i, carry):
        part = pl.ds(pl.multiple_of(i * step, step), step)
        v = tok_ref[part, :].astype(jnp.float32)
        r = lax.rsqrt(jnp.mean(v * v, axis=-1, keepdims=True) + NORM_EPSILON)
        n = (v * r * gain_ref[...]).astype(jnp.bfloat16)
        for q in range(tp_count):
            x_buf[e, q, part, :] = n[:, q * quarter : (q + 1) * quarter]
        return carry

    lax.fori_loop(0, rows // step, norm_rows, 0)
    pl.semaphore_wait(barrier, ep_count + tp_count - 2)

    def wt_copy(k, slot, who):
        src = wt_ref if slot is None else wt_all.at[slot]
        dst = wt_all.at[e if slot is None else slot]
        return remote(src, dst, wt_s.at[k], wt_r.at[k], {"ep": who})

    def head_of(g, q):
        return x_buf.at[g, q, :, head_cols]

    def rest_of(g, q):
        return x_buf.at[g, q, :, rest_cols]

    def line_head(g, s, who):
        return (remote(head_of(g, t), head_of(g, t), s.at[g, 0], z_r.at[g, 0], who),)

    def line_rest(g, s, who):
        return (
            remote(rest_of(g, t), rest_of(g, t), s.at[g, 1], z_r.at[g, 1], who),
            remote(rest_of(g, t2), rest_of(g, t2), s.at[g, 2], z_r.at[g, 2], who),
        )

    def y_copy_head(g):
        return remote(head_of(g, t), head_of(g, t), ya_s.at[g], ya_r.at[g], mate_y)

    def x_copy(g):
        ref = x_buf.at[g, t, :, head_cols]
        return remote(ref, ref, x_s.at[g], x_r.at[g], mate_x)

    def x_arrival(g):
        ref = x_buf.at[g, t2, :, head_cols]
        return remote(ref, ref, x_s.at[g], x_r.at[g], mate_x)

    def c_copies(g, lane):
        main, other = 2 * xi + lane, 2 * (1 - xi) + lane
        refs = (head_of(g, main), rest_of(g, main), rest_of(g, other), head_of(g, other))
        return [remote(r, r, c_s.at[g, i], c_r.at[g, i], mate_c) for i, r in enumerate(refs)]

    def order(j):
        k = jnp.minimum(z, major - 1 - z)
        d = (j + 1) // 2
        near = jnp.where(j % 2 == 1, z - d, z + d)
        far = jnp.where(z <= major - 1 - z, j, major - 1 - j)
        return jnp.where(j <= 2 * k, near, far)

    def slot_group(i):
        p = order(i // 2)
        yy = jnp.where(i % 2 == 0, y, 1 - y)
        return p, p * minor + yy

    def forward(p, g, pieces):
        @pl.when((p <= z) & (z < major - 1))
        def _():
            for copy in pieces(g, u_s, z_up):
                copy.start()

        @pl.when((p >= z) & (z > 0))
        def _():
            for copy in pieces(g, d_s, z_down):
                copy.start()

    for copy in line_rest(e, y_s, mate_y):
        copy.start()
    forward(z, e, line_head)
    y_copy_head(e).start()
    for k in range(1, ep_count):
        wt_copy(k, None, lax.rem(e + k, ep_count)).start()
    wt_all[e] = wt_ref[...]
    forward(z, e, line_rest)

    loads[0].wait()
    loads[1].wait()
    sg_sum = jnp.zeros((rows, sg.shape[1]), jnp.float32)
    su_sum = jnp.zeros((rows, sg.shape[1]), jnp.float32)
    for q in range(tp_count):
        band = pl.ds(q * quarter, quarter)
        sg_sum += jnp.dot(x_buf[e, q], sg[band, :], preferred_element_type=jnp.float32)
        su_sum += jnp.dot(x_buf[e, q], su[band, :], preferred_element_type=jnp.float32)
    sh_all[t] = (silu(sg_sum) * su_sum).astype(jnp.bfloat16)

    def sh_copy(k, slot, who):
        return remote(sh_all.at[slot], sh_all.at[slot], sh_s.at[k], sh_r.at[k], {"tp": who})

    for k in range(1, tp_count):
        sh_copy(k, t, lax.rem(t + k, tp_count)).start()
    for load in loads[2:5]:
        load.wait()
    for k in range(1, ep_count):
        wt_copy(k, lax.rem(e + ep_count - k, ep_count), e).wait_recv()

    expert = e * (tp_count // 2) + xi
    expert_mask = lax.broadcasted_iota(jnp.int32, wt_ref.shape, 0) == expert
    eye = lax.broadcasted_iota(jnp.int32, (rows, rows), 0) == lax.broadcasted_iota(
        jnp.int32, (rows, rows), 1
    )

    def compute(g):
        row = jnp.sum(jnp.where(expert_mask, wt_all[g], 0.0), axis=0, keepdims=True)
        weight = jnp.sum(jnp.where(eye, row, 0.0), axis=1, keepdims=True)
        ff = gate.shape[1]
        g_sum = jnp.zeros((rows, ff), jnp.float32)
        u_sum = jnp.zeros((rows, ff), jnp.float32)
        for q in range(tp_count):
            band = pl.ds(q * quarter, quarter)
            g_sum += jnp.dot(x_buf[g, q], gate[band, :], preferred_element_type=jnp.float32)
            u_sum += jnp.dot(x_buf[g, q], up[band, :], preferred_element_type=jnp.float32)
        act = (silu(g_sum) * u_sum).astype(jnp.bfloat16)
        for q in range(tp_count):
            part = jnp.dot(
                act, down[:, q * quarter : (q + 1) * quarter], preferred_element_type=jnp.float32
            )
            y_buf[g, q] = (part * weight).astype(jnp.bfloat16)

    def yc_copy(g, k):
        return remote(
            y_buf.at[g, 2 * k + 1 - c], c_buf.at[g, k], yc_s.at[g, k], yc_r.at[g, k], mate_c
        )

    def rx_copy(g):
        return remote(xs_buf.at[g], xr_buf.at[g], rx_s.at[g], rx_r.at[g], mate_x)

    def rya_copy(p):
        return remote(ysa_buf.at[p], yra_buf.at[p], rya_s.at[p], rya_r.at[p], mate_y)

    total = ep_count

    def head_sum(g):
        return (
            y_buf[g, t, :, head_cols].astype(jnp.float32)
            + c_buf[g, xi, :, head_cols].astype(jnp.float32)
            + xr_buf[g].astype(jnp.float32)
        )

    def main_step(i, carry):
        @pl.when((i >= 1) & (i < total))
        def _():
            p, g = slot_group(i)
            ours = c_copies(g, c)

            @pl.when(i % 2 == 0)
            def _():
                line_head(g, u_s, z_up)[0].wait_recv()
                forward(p, g, line_head)
                y_copy_head(g).start()
                x_copy(g).start()
                ours[0].start()

            for copy in line_rest(g, u_s, z_up):
                copy.wait_recv()
            forward(p, g, line_rest)
            ours[1].start()
            ours[2].start()

        @pl.when((i >= 2) & (i <= total) & (i % 2 == 0))
        def _():
            _, g = slot_group(i - 1)
            y_copy_head(g).wait_recv()
            x_copy(g).start()
            c_copies(g, c)[0].start()

        @pl.when((i >= 4) & (i <= total + 2))
        def _():
            _, g = slot_group(i - 3)
            x_arrival(g).wait_recv()
            c_copies(g, c)[3].start()

        @pl.when((i >= 4) & (i <= total + 3))
        def _():
            _, g = slot_group(i - 4)

            @pl.when(i >= 5)
            def _():
                for copy in c_copies(g, 1 - c):
                    copy.wait_recv()

            compute(g)
            for k in range(2):
                yc_copy(g, k).start()

        @pl.when((i >= 5) & (i <= total + 4))
        def _():
            _, g = slot_group(i - 5)
            for k in range(2):
                yc_copy(g, k).wait_recv()
            xs_buf[g] = (
                y_buf[g, t2, :, head_cols].astype(jnp.float32)
                + c_buf[g, 1 - xi, :, head_cols].astype(jnp.float32)
            ).astype(jnp.bfloat16)
            rx_copy(g).start()

        @pl.when((i >= 8) & (i % 2 == 0))
        def _():
            p, g = slot_group(i - 7)
            rx_copy(g).wait_recv()
            ysa_buf[p] = head_sum(g).astype(jnp.bfloat16)
            rya_copy(p).start()

        return carry

    lax.fori_loop(0, total + 7, main_step, 0)

    loads[5].wait()
    for k in range(1, tp_count):
        sh_copy(k, lax.rem(t + tp_count - k, tp_count), t).wait_recv()
    shared = jnp.zeros((rows, quarter), jnp.float32)
    width = sg.shape[1]
    for q in range(tp_count):
        shared += jnp.dot(
            sh_all[q], sd[q * width : (q + 1) * width, :], preferred_element_type=jnp.float32
        )
    sh_out[...] = shared

    def rz_copy(g, lane, who):
        return remote(zs_buf.at[g], zr_buf.at[lane, g], rz_s.at[g], rz_r.at[lane, g], who)

    def rza_copy(p, lane, who):
        return remote(zsa_buf.at[p], zra_buf.at[lane, p], rza_s.at[p], rza_r.at[lane, p], who)

    def sum_rest(p, g):
        acc[:, split:quarter] = y_buf[g, t, :, rest_cols].astype(jnp.float32) + c_buf[
            g, xi, :, rest_cols
        ].astype(jnp.float32)
        acc[:, quarter:] = y_buf[g, t2, :, rest_cols].astype(jnp.float32) + c_buf[
            g, 1 - xi, :, rest_cols
        ].astype(jnp.float32)

        @pl.when((p >= z) & (z > 0))
        def _():
            rz_copy(g, 0, z_up).wait_recv()
            acc[:, split:] += zr_buf[0, g].astype(jnp.float32)

        @pl.when((p <= z) & (z < major - 1))
        def _():
            rz_copy(g, 1, z_up).wait_recv()
            acc[:, split:] += zr_buf[1, g].astype(jnp.float32)

    def sum_head(p, g):
        rx_copy(g).wait_recv()
        rya_copy(p).wait_recv()
        acc[:, :split] = head_sum(g) + yra_buf[p].astype(jnp.float32)

        @pl.when((p >= z) & (z > 0))
        def _():
            rza_copy(p, 0, z_up).wait_recv()
            acc[:, :split] += zra_buf[0, p].astype(jnp.float32)

        @pl.when((p <= z) & (z < major - 1))
        def _():
            rza_copy(p, 1, z_up).wait_recv()
            acc[:, :split] += zra_buf[1, p].astype(jnp.float32)

    def sum_step(q, carry):
        ups = major - 1 - z
        low = jnp.where(q < ups, z + 1 + q, z - 1 - (q - ups))
        high = jnp.where(q < z, z - 1 - q, z + 1 + (q - z))
        p = jnp.where(2 * z < major, low, high)

        def send(copy, key):
            @pl.when(p > z)
            def _():
                copy(key, 0, z_up).start()

            @pl.when(p < z)
            def _():
                copy(key, 1, z_down).start()

        for yy in (1 - y, y):
            g = p * minor + yy
            sum_rest(p, g)
            zs_buf[g] = acc[:, split:].astype(jnp.bfloat16)
            send(rz_copy, g)
        sum_head(p, p * minor + y)
        zsa_buf[p] = acc[:, :split].astype(jnp.bfloat16)
        send(rza_copy, p)
        return carry

    lax.fori_loop(0, major - 1, sum_step, 0)

    y_copy = remote(ys_buf, yr_buf, ry_s, ry_r, mate_y)
    sum_rest(z, z * minor + 1 - y)
    ys_buf[...] = acc[:, split:].astype(jnp.bfloat16)
    y_copy.start()
    sum_rest(z, e)
    sum_head(z, e)
    y_copy.wait_recv()
    acc[:, split:] += yr_buf[...].astype(jnp.float32)
    final = acc[...]
    f_copy = remote(fs_buf, fr_buf, f_s, f_r, mate_x)
    fs_buf[...] = final[:, quarter:].astype(jnp.bfloat16)
    f_copy.start()
    out_ref[:, :split] = (final[:, :split] + sh_out[:, :split]).astype(jnp.bfloat16)
    f_copy.wait_recv()
    out_ref[:, split:] = (
        final[:, split:quarter] + fr_buf[...].astype(jnp.float32) + sh_out[:, split:]
    ).astype(jnp.bfloat16)

    f_copy.wait_send()
    y_copy.wait_send()
    for copy in line_rest(e, y_s, mate_y):
        copy.wait_send()
    for k in range(1, ep_count):
        wt_copy(k, None, lax.rem(e + k, ep_count)).wait_send()
    for k in range(1, tp_count):
        sh_copy(k, t, lax.rem(t + k, tp_count)).wait_send()

    def drain(i, carry):
        p, g = slot_group(i)

        def sent(pieces):
            @pl.when((p <= z) & (z < major - 1))
            def _():
                for copy in pieces(g, u_s, z_up):
                    copy.wait_send()

            @pl.when((p >= z) & (z > 0))
            def _():
                for copy in pieces(g, d_s, z_down):
                    copy.wait_send()

        sent(line_rest)

        @pl.when(i % 2 == 0)
        def _():
            sent(line_head)
            y_copy_head(g).wait_send()

            @pl.when(p != z)
            def _():
                rza_copy(p, 0, z_up).wait_send()

        @pl.when(i % 2 == 1)
        def _():
            rya_copy(p).wait_send()

        @pl.when(i > 0)
        def _():
            x_copy(g).wait_send()
            for copy in c_copies(g, c):
                copy.wait_send()

        for k in range(2):
            yc_copy(g, k).wait_send()
        rx_copy(g).wait_send()

        @pl.when(p != z)
        def _():
            rz_copy(g, 0, z_up).wait_send()

        return carry

    lax.fori_loop(0, total, drain, 0)


def dense_exchange(
    tokens, norm_gain, expert_ids, route_weights, expert_gate, expert_up, expert_down,
    shared_gate, shared_up, shared_down,
):
    ep_count = lax.axis_size("ep")
    tp_count = lax.axis_size("tp")
    minor = 1 << (ep_count.bit_length() - 1) // 2
    rows, width = tokens.shape
    quarter = width // tp_count
    split = quarter * 3 // 4 // LANES * LANES
    expert_count = ep_count * tp_count // 2
    wide = quarter + quarter - split
    expert_iota = jnp.arange(expert_count, dtype=jnp.int32)
    table = jnp.sum(
        jnp.where(
            expert_ids[None, :, :] == expert_iota[:, None, None], route_weights[None, :, :], 0.0
        ),
        axis=2,
    )
    ff = expert_gate.shape[2]
    share = shared_gate.shape[1]
    bf16, f32 = jnp.bfloat16, jnp.float32
    dma = pltpu.SemaphoreType.DMA
    vmem = pl.BlockSpec(memory_space=pltpu.VMEM)
    anywhere = pl.BlockSpec(memory_space=pl.ANY)
    n = ep_count
    major = n // minor
    return pl.pallas_call(
        functools.partial(dense_kernel, ep_count, tp_count, minor, split),
        out_shape=jax.ShapeDtypeStruct((rows, quarter), bf16),
        in_specs=[vmem] * 3 + [anywhere] * 6,
        out_specs=vmem,
        scratch_shapes=[
            pltpu.VMEM((n, tp_count, rows, quarter), bf16),
            pltpu.VMEM((n, tp_count, rows, quarter), bf16),
            pltpu.VMEM((n, 2, rows, quarter), bf16),
            pltpu.VMEM((n, rows, split), bf16),
            pltpu.VMEM((n, rows, split), bf16),
            pltpu.VMEM((major, rows, split), bf16),
            pltpu.VMEM((major, rows, split), bf16),
            pltpu.VMEM((major, rows, split), bf16),
            pltpu.VMEM((2, major, rows, split), bf16),
            pltpu.VMEM((n, rows, wide - split), bf16),
            pltpu.VMEM((2, n, rows, wide - split), bf16),
            pltpu.VMEM((rows, wide - split), bf16),
            pltpu.VMEM((rows, wide - split), bf16),
            pltpu.VMEM((rows, quarter - split), bf16),
            pltpu.VMEM((rows, quarter - split), bf16),
            pltpu.VMEM((rows, wide), f32),
            pltpu.VMEM((n, expert_count, rows), f32),
            pltpu.VMEM((tp_count, rows, share), bf16),
            pltpu.VMEM((rows, quarter), f32),
            pltpu.VMEM((width, ff), bf16),
            pltpu.VMEM((width, ff), bf16),
            pltpu.VMEM((ff, width), bf16),
            pltpu.VMEM((width, share), bf16),
            pltpu.VMEM((width, share), bf16),
            pltpu.VMEM((share * tp_count, quarter), bf16),
            dma((6,)), dma((n,)), dma((n,)), dma((tp_count,)), dma((tp_count,)),
            dma((n, 3)), dma((n, 3)), dma((n, 3)), dma((n, 3)),
            dma((n,)), dma((n,)), dma((n, 4)), dma((n, 4)), dma((n,)), dma((n,)),
            dma((n, 2)), dma((n, 2)), dma((n,)), dma((n,)), dma((major,)), dma((major,)),
            dma((major,)), dma((2, major)), dma((n,)), dma((2, n)), dma, dma, dma, dma,
        ],
        compiler_params=pltpu.CompilerParams(
            collective_id=0, has_side_effects=True, vmem_limit_bytes=60 << 20
        ),
        name="dense_moe",
    )(
        tokens, norm_gain.reshape(1, width), table, expert_gate[0], expert_up[0], expert_down[0],
        shared_gate, shared_up, shared_down,
    )


def local(tokens, *rest):
    ep_count = lax.axis_size("ep")
    pair_count = lax.axis_size("tp") // 2
    dense_bytes = 4 * ep_count * tokens.size * tokens.dtype.itemsize
    minor = 1 << (ep_count.bit_length() - 1) // 2
    if pair_count == 2 and minor == 2 and dense_bytes <= 24 << 20:
        return dense_exchange(tokens, *rest)
    return routed_exchange(tokens, *rest)


def solution(mesh):
    return jax.shard_map(
        local,
        mesh=mesh,
        in_specs=(
            P("ep", None),
            P(),
            P("ep", None),
            P("ep", None),
            P(("ep", "tp"), None, None),
            P(("ep", "tp"), None, None),
            P(("ep", "tp"), None, None),
            P(None, "tp"),
            P(None, "tp"),
            P(None, "tp"),
        ),
        out_specs=P("ep", "tp"),
        check_vma=False,
    )
```

profile of v0, /device:TPU:0, one launch (start us, length us, event | category | flops | bytes accessed | tf_op | source)
XLA Modules:
  0.0 84.0 jit_solution(7822648755241324073)
XLA Ops:
  0.0 0.0 copy-start
  0.0 0.7 copy-done
  0.7 1.3 %select_reduce_fusion.wt_ref = f32[16,128]{1,0:T(8,128)} fusion(f32[128,6]{0,1:T(8,128)S(1)} %copy-done, s32[128,6]{0,1:T(8,128)} %param.12), kind=kLoop, calls=%fused_computation | loop fusion | flops 34816 | bytes 14336 | tf_op jit(solution)/shard_map/reduce_sum | solution.py:551
  2.0 80.5 %dense_moe.1 = bf16[128,512]{1,0:T(8,128)(2,1)} custom-call(bf16[128,2048]{1,0:T(8,128)(2,1)} %tok_ref.1, f32[1,2048]{1,0:T(1,128)} %bitcast.7, f32[16,128]{1,0:T(8,128)} %select_reduce_fusion.wt_ref, bf16[2048,256]{1,0:T(8,128)(2,1)} %bitcast.4, bf16[2048,256]{1,0:T(8,128)(2,1)} %bitcast.5, bf16[256,2048]{1,0:T(8,128)(2,1)} %bitcast.6, ...), custom_call_target="tpu_custom_call" | custom-call | tf_op jit(solution)/shard_map/dense_moe/pallas_call | solution.py:565
  82.5 1.6 %copy.14 = bf16[128,512]{1,0:T(8,128)(2,1)} copy(bf16[128,512]{1,0:T(8,128)(2,1)} %dense_moe.1) | data formatting | bytes 262144
Async XLA Ops:
  0.0 0.7 copy-start
where the time goes:
time: 84.2 us; the launch traced here: 84 us
  Pallas kernels  80.5 us (96%)
  local copies, waits for them, and re-layouts  2.25 us (3%)
  other arithmetic  1.3 us (2%)
    pallas_call x1, Pallas kernels, dense_exchange(): pl.pallas_call(functools.partial(dense_kernel, ep_count, tp_count, minor,...  80.5 us
    unnamed x3, local copies, waits for them, and re-layouts  2.25 us

commit v1 on v0

v1 whole, which is shorter than its diff:
```python
import functools

import jax
import jax.numpy as jnp
from jax import lax
from jax.experimental import pallas as pl
from jax.experimental.pallas import tpu as pltpu
from jax.sharding import PartitionSpec as P

NORM_EPSILON = 1e-06


def swapped(block, axis, distance):
    count = lax.axis_size(axis)
    route = []
    for low in range(count):
        high = low | 1 << distance
        if high != low and high < count:
            route += [(low, high), (high, low)]
    return lax.ppermute(block, axis, route)


def routed_exchange(
    tokens,
    norm_gain,
    expert_ids,
    route_weights,
    expert_gate,
    expert_up,
    expert_down,
    shared_gate,
    shared_up,
    shared_down,
):
    ep_count = lax.axis_size("ep")
    tp_count = lax.axis_size("tp")
    pair_count = tp_count // 2
    tp_index = lax.axis_index("tp")
    column = tp_index // 2
    half_index = tp_index % 2
    token_count, model_width = tokens.shape
    top_count = expert_ids.shape[1]
    expert_count = ep_count * pair_count
    capacity = 2 * max(1, token_count * top_count // expert_count)
    half_cap = capacity // 2
    as_float = tokens.astype(jnp.float32)
    inverse_rms = lax.rsqrt(jnp.mean(as_float * as_float, axis=-1, keepdims=True) + NORM_EPSILON)
    normed = (as_float * inverse_rms * norm_gain).astype(jnp.bfloat16)
    expert_iota = jnp.arange(expert_count, dtype=jnp.int32)
    token_iota = jnp.arange(token_count, dtype=jnp.int32)
    counts = jnp.sum(
        (expert_ids[:, :, None] == expert_iota[None, None, :]).astype(jnp.bfloat16), axis=1
    )
    strict_lower = (token_iota[:, None] > token_iota[None, :]).astype(jnp.bfloat16)
    prefix = jnp.dot(strict_lower, counts, preferred_element_type=jnp.float32)
    slot_index = jnp.take_along_axis(prefix, expert_ids, axis=1).astype(jnp.int32)
    target = expert_ids // pair_count
    owner_column = expert_ids % pair_count
    is_mine = owner_column == column
    position = target * capacity + slot_index
    slot_iota = jnp.arange(ep_count * capacity, dtype=jnp.int32)
    matches = is_mine[None, :, :] & (position[None, :, :] == slot_iota[:, None, None])
    slot_taken = jnp.any(matches, axis=2)
    token_of_slot = jnp.sum(jnp.where(slot_taken, token_iota[None, :], 0), axis=1)
    filled = jnp.any(slot_taken, axis=1)
    buffer = jnp.where(
        filled[:, None], jnp.take(normed, token_of_slot, axis=0), jnp.zeros((), jnp.bfloat16)
    )
    buffer = buffer.reshape(ep_count, capacity, model_width)
    gate_local = expert_gate[0]
    up_local = expert_up[0]
    down_local = expert_down[0]
    received = lax.all_to_all(buffer, "ep", split_axis=0, concat_axis=0, tiled=True)
    flat_rows = received.reshape(-1, model_width)
    hidden = (
        jax.nn.silu(jnp.dot(flat_rows, gate_local, preferred_element_type=jnp.float32))
        * jnp.dot(flat_rows, up_local, preferred_element_type=jnp.float32)
    ).astype(jnp.bfloat16)
    partial_out = jnp.dot(hidden, down_local, preferred_element_type=jnp.float32).astype(
        jnp.bfloat16
    )
    partial_out = partial_out.reshape(received.shape[0], received.shape[1], model_width)
    kept_part = lax.dynamic_slice_in_dim(partial_out, half_index * half_cap, half_cap, 1)
    other_part = lax.dynamic_slice_in_dim(partial_out, (1 - half_index) * half_cap, half_cap, 1)
    partner_part = swapped(other_part, "tp", 0)
    expert_out = (kept_part.astype(jnp.float32) + partner_part.astype(jnp.float32)).astype(
        jnp.bfloat16
    )
    returned = lax.all_to_all(expert_out, "ep", split_axis=0, concat_axis=0, tiled=True)
    row_total = ep_count * half_cap
    flat_rows = returned.reshape(row_total, model_width).astype(jnp.float32)
    is_valid = is_mine & (slot_index // half_cap == half_index)
    row_index = jnp.where(is_valid, target * half_cap + slot_index % half_cap, -1)
    row_iota = jnp.arange(row_total, dtype=jnp.int32)
    hits = row_index[:, :, None] == row_iota[None, None, :]
    combine_table = jnp.sum(jnp.where(hits, route_weights[:, :, None], 0.0), axis=1)
    partial_routed = jnp.dot(
        combine_table,
        flat_rows,
        precision=lax.Precision.HIGHEST,
        preferred_element_type=jnp.float32,
    )
    routed = lax.psum_scatter(partial_routed, "tp", scatter_dimension=1, tiled=True)
    shared_act = (
        jax.nn.silu(jnp.dot(normed, shared_gate, preferred_element_type=jnp.float32))
        * jnp.dot(normed, shared_up, preferred_element_type=jnp.float32)
    ).astype(jnp.bfloat16)
    shared_out = jnp.dot(
        lax.all_gather(shared_act, "tp", axis=1, tiled=True),
        shared_down,
        preferred_element_type=jnp.float32,
    )
    return (routed + shared_out).astype(jnp.bfloat16)


MESH = pl.DeviceIdType.MESH
LANES = 128
KEEP = 6
NEAR = 6
TURN = 2
LAG = 2


def silu(v):
    return v / (1.0 + jnp.exp(-v))


def dense_kernel(
    ep_count, tp_count, minor, near, keep, lag, turn,
    ids_ref, rw_ref, gain_ref, tok_hbm, gate_hbm, up_hbm, down_hbm, sg_hbm, su_hbm, sd_hbm,
    out_ref,
    tok, xb, xo, wtab, wr, wg, wu, wd, sg, su, sd, sh_all, sh_out,
    pa, pb, xs, xr, ys, yr, zas, zar, zbs, zbr, fs, fr, fin, fin_in, acc_a, acc_b,
    load_sem, wt_s, wt_r, we_s, we_r, sh_s, sh_r, yb_s,
    au_s, ad_s, a_r, bu_s, bd_s, b_r, ya_s, ya_r, xa_s, xa_r,
    rx_s, rx_r, ry_s, ry_r, rza_s, rza_r, rzb_s, rzb_r, f_s, f_r, o_s, o_r,
):
    n = ep_count
    major = n // minor
    half, width = xo.shape
    side = width // 2
    quarter = width // tp_count
    tail = side - keep
    e = lax.axis_index("ep")
    t = lax.axis_index("tp")
    z = e // minor
    y = e % minor
    xi = t // 2
    c = t % 2
    t2 = 2 * (1 - xi) + c
    other_y = z * minor + 1 - y
    mate_x = {"tp": t2}
    mate_c = {"tp": 2 * xi + 1 - c}
    mate_y = {"ep": other_y}
    across = {"ep": other_y, "tp": t2}
    z_up = {"ep": lax.rem(e + minor, n)}
    z_down = {"ep": lax.rem(e + n - minor, n)}
    is_end = (z == 0) | (z == major - 1)

    barrier = pltpu.get_barrier_semaphore()
    for k in range(1, n):
        pl.semaphore_signal(barrier, inc=1, device_id={"ep": lax.rem(e + k, n)}, device_id_type=MESH)
    for k in range(1, tp_count):
        pl.semaphore_signal(barrier, inc=1, device_id={"tp": lax.rem(t + k, tp_count)}, device_id_type=MESH)
    pl.semaphore_signal(barrier, inc=1, device_id=across, device_id_type=MESH)

    def remote(src, dst, s, r, who):
        return pltpu.make_async_remote_copy(
            src_ref=src, dst_ref=dst, send_sem=s, recv_sem=r, device_id=who, device_id_type=MESH
        )

    def rows_of(which):
        return pl.ds(pl.multiple_of(which * half, half), half)

    def side_of(which):
        return pl.ds(pl.multiple_of(which * side, side), side)

    loads = [
        pltpu.make_async_copy(a, b, load_sem.at[i])
        for i, (a, b) in enumerate(
            (
                (tok_hbm.at[rows_of(c)], tok.at[0]),
                (tok_hbm.at[rows_of(1 - c)], tok.at[1]),
                (gate_hbm, wg.at[c]),
                (up_hbm, wu.at[c]),
                (down_hbm.at[:, side_of(xi)], wd.at[c, :, pl.ds(0, side)]),
                (down_hbm.at[:, side_of(1 - xi)], wd.at[c, :, pl.ds(side, side)]),
                (sg_hbm, sg),
                (su_hbm, su),
                (sd_hbm, sd),
            )
        )
    ]
    for load in loads:
        load.start()

    step = 16

    def norm_into(which, store):
        def body(i, carry):
            part = pl.ds(pl.multiple_of(i * step, step), step)
            v = tok[which, part, :].astype(jnp.float32)
            r = lax.rsqrt(jnp.mean(v * v, axis=-1, keepdims=True) + NORM_EPSILON)
            store(part, (v * r * gain_ref[...]).astype(jnp.bfloat16))
            return carry

        lax.fori_loop(0, half // step, body, 0)

    def store_own(part, value):
        xb[e, part, :] = value

    def store_rest(part, value):
        xo[part, :] = value

    def weights_for(expert):
        row = jnp.zeros((1, ids_ref.shape[1]), jnp.float32)
        for k in range(ids_ref.shape[0]):
            row += jnp.where(ids_ref[k : k + 1, :] == expert, rw_ref[k : k + 1, :], 0.0)
        return row

    loads[0].wait()
    norm_into(0, store_own)
    for d in range(n):
        wtab[d] = weights_for(d * (tp_count // 2) + xi)
    wr[e] = weights_for(e * (tp_count // 2) + xi)
    pl.semaphore_wait(barrier, n + tp_count - 1)

    mine = pl.ds(pl.multiple_of(xi * near, LANES), near)
    theirs = pl.ds(pl.multiple_of((1 - xi) * near, LANES), near)
    rest = pl.ds(2 * near, width - 2 * near)

    def line_a(g, s, who):
        ref = xb.at[g, :, mine]
        return remote(ref, ref, s.at[g], a_r.at[g], who)

    def line_b(g, s, who):
        ref = xb.at[g, :, rest]
        return remote(ref, ref, s.at[g], b_r.at[g], who)

    def y_first():
        ref = xb.at[e, :, rest]
        return remote(ref, ref, yb_s, b_r.at[e], mate_y)

    def y_copy(g):
        ref = xb.at[g, :, mine]
        return remote(ref, ref, ya_s.at[g], ya_r.at[g], mate_y)

    def x_copy(g):
        ref = xb.at[g, :, mine]
        return remote(ref, ref, xa_s.at[g], xa_r.at[g], mate_x)

    def x_arrival(g):
        ref = xb.at[g, :, theirs]
        return remote(ref, ref, xa_s.at[g], xa_r.at[g], mate_x)

    def wt_copy(k, target):
        return remote(wtab.at[target], wr.at[e], wt_s.at[k], wt_r.at[e], {"ep": target})

    def wt_arrival(g):
        return remote(wtab.at[g], wr.at[g], wt_s.at[0], wt_r.at[g], mate_y)

    def weight_copy(i, which):
        ref = (wg, wu, wd)[i].at[which]
        return remote(ref, ref, we_s.at[i], we_r.at[i], mate_c)

    def sh_copy(k, slot, who):
        return remote(sh_all.at[slot], sh_all.at[slot], sh_s.at[k], sh_r.at[k], {"tp": who})

    def order(j):
        k = jnp.minimum(z, major - 1 - z)
        d = (j + 1) // 2
        close = jnp.where(j % 2 == 1, z - d, z + d)
        far = jnp.where(z <= major - 1 - z, j, major - 1 - j)
        return jnp.where(j <= 2 * k, close, far)

    def slot_group(i):
        p = order(i // 2)
        yy = jnp.where(i % 2 == 0, y, 1 - y)
        return p, p * minor + yy

    def ups(p):
        return (p <= z) & (z < major - 1)

    def downs(p):
        return (p >= z) & (z > 0)

    def forward(p, g, line, s_up, s_down):
        @pl.when(ups(p))
        def _():
            line(g, s_up, z_up).start()

        @pl.when(downs(p))
        def _():
            line(g, s_down, z_down).start()

    forward(z, e, line_a, au_s, ad_s)
    y_first().start()
    y_copy(e).start()
    forward(z, e, line_b, bu_s, bd_s)
    for k in range(1, n):
        wt_copy(k, lax.rem(e + k, n)).start()
    loads[2].wait()
    weight_copy(0, c).start()
    loads[3].wait()
    weight_copy(1, c).start()
    loads[4].wait()
    loads[5].wait()
    weight_copy(2, c).start()
    loads[1].wait()
    norm_into(1, store_rest)
    loads[6].wait()
    loads[7].wait()

    def shared_in(x):
        g_sum = jnp.dot(x, sg[...], preferred_element_type=jnp.float32)
        u_sum = jnp.dot(x, su[...], preferred_element_type=jnp.float32)
        return (silu(g_sum) * u_sum).astype(jnp.bfloat16)

    sh_all[t, c] = shared_in(xb[e])
    sh_all[t, 1 - c] = shared_in(xo[...])
    for k in range(1, tp_count):
        sh_copy(k, t, lax.rem(t + k, tp_count)).start()

    def rx_copy(g):
        return remote(xs.at[g], xr.at[g], rx_s.at[g], rx_r.at[g], mate_x)

    def ry_copy(p):
        return remote(ys.at[p], yr.at[p], ry_s.at[p], ry_r.at[p], mate_y)

    def rza_copy(p, lane, who):
        return remote(zas.at[p], zar.at[lane, p], rza_s.at[p], rza_r.at[lane, p], who)

    def rzb_copy(g, lane, who):
        return remote(zbs.at[g], zbr.at[lane, g], rzb_s.at[g], rzb_r.at[lane, g], who)

    diagonal = lax.broadcasted_iota(jnp.int32, (half, 2 * half), 1) == (
        lax.broadcasted_iota(jnp.int32, (half, 2 * half), 0) + c * half
    )

    def compute(g):
        weight = jnp.sum(jnp.where(diagonal, wr[g], 0.0), axis=1, keepdims=True)
        x = xb[g]
        acts = []
        for h in range(2):
            g_sum = jnp.dot(x, wg[h], preferred_element_type=jnp.float32)
            u_sum = jnp.dot(x, wu[h], preferred_element_type=jnp.float32)
            acts.append((silu(g_sum) * u_sum).astype(jnp.bfloat16))

        def columns(low, high):
            total = jnp.dot(acts[0], wd[0, :, low:high], preferred_element_type=jnp.float32)
            total += jnp.dot(acts[1], wd[1, :, low:high], preferred_element_type=jnp.float32)
            return total * weight

        xs[g] = columns(side, side + keep).astype(jnp.bfloat16)
        rx_copy(g).start()
        pa[g] = columns(0, keep)
        pb[g, :, :tail] = columns(keep, side)
        pb[g, :, tail:] = columns(side + keep, width)

    def sum_b(p, g):
        acc_b[...] = pb[g]

        @pl.when(downs(p))
        def _():
            rzb_copy(g, 0, z_up).wait_recv()
            acc_b[...] += zbr[0, g].astype(jnp.float32)

        @pl.when(ups(p))
        def _():
            rzb_copy(g, 1, z_up).wait_recv()
            acc_b[...] += zbr[1, g].astype(jnp.float32)

    def sum_a(p, g):
        rx_copy(g).wait_recv()
        ry_copy(p).wait_recv()
        acc_a[...] = pa[g] + xr[g].astype(jnp.float32) + yr[p].astype(jnp.float32)

        @pl.when(downs(p))
        def _():
            rza_copy(p, 0, z_up).wait_recv()
            acc_a[...] += zar[0, p].astype(jnp.float32)

        @pl.when(ups(p))
        def _():
            rza_copy(p, 1, z_up).wait_recv()
            acc_a[...] += zar[1, p].astype(jnp.float32)

    def line_sums(p):
        def send(copy, key):
            @pl.when(p > z)
            def _():
                copy(key, 0, z_up).start()

            @pl.when(p < z)
            def _():
                copy(key, 1, z_down).start()

        for yy in (1 - y, y):
            g = p * minor + yy
            sum_b(p, g)
            zbs[g] = acc_b[...].astype(jnp.bfloat16)
            send(rzb_copy, g)
        sum_a(p, p * minor + y)
        zas[p] = acc_a[...].astype(jnp.bfloat16)
        send(rza_copy, p)

    def main_step(i, carry):
        @pl.when((i >= 1) & (i < n))
        def _():
            p, g = slot_group(i)

            @pl.when(i % 2 == 0)
            def _():
                line_a(g, au_s, z_up).wait_recv()
                forward(p, g, line_a, au_s, ad_s)
                y_copy(g).start()
                x_copy(g).start()

            line_b(g, bu_s, z_up).wait_recv()
            forward(p, g, line_b, bu_s, bd_s)

        @pl.when((i >= 2) & (i <= n) & (i % 2 == 0))
        def _():
            _, g = slot_group(i - 1)
            y_copy(g).wait_recv()
            x_copy(g).start()

        @pl.when(i == lag)
        def _():
            for j in range(3):
                weight_copy(j, 1 - c).wait_recv()

        @pl.when((i >= lag) & (i < n + lag))
        def _():
            _, g = slot_group(i - lag)

            @pl.when(i > lag)
            def _():
                x_arrival(g).wait_recv()
                wt_arrival(g).wait_recv()

            compute(g)

        @pl.when(i == n)
        def _():
            loads[8].wait()
            for k in range(1, tp_count):
                sh_copy(k, lax.rem(t + tp_count - k, tp_count), t).wait_recv()
            share = sg.shape[1]
            for r in range(2):
                shared = jnp.zeros((half, quarter), jnp.float32)
                for q in range(tp_count):
                    shared += jnp.dot(
                        sh_all[q, r], sd[q * share : (q + 1) * share, :],
                        preferred_element_type=jnp.float32,
                    )
                sh_out[r] = shared

        @pl.when((i >= lag + turn + 1) & (i < n + lag + turn) & ((i - lag - turn) % 2 == 1))
        def _():
            p, g = slot_group(i - lag - turn)
            rx_copy(g).wait_recv()
            ys[p] = (pa[g] + xr[g].astype(jnp.float32)).astype(jnp.bfloat16)
            ry_copy(p).start()

        @pl.when(is_end & (i >= lag + turn + 4) & ((i - lag - turn) % 2 == 0))
        def _():
            line_sums(order((i - lag - turn - 2) // 2))

        return carry

    lax.fori_loop(0, n + lag + turn + 1, main_step, 0)

    @pl.when(jnp.logical_not(is_end))
    def _():
        def sum_step(q, carry):
            above = major - 1 - z
            low = jnp.where(q < above, z + 1 + q, z - 1 - (q - above))
            high = jnp.where(q < z, z - 1 - q, z + 1 + (q - z))
            line_sums(jnp.where(2 * z < major, low, high))
            return carry

        lax.fori_loop(0, major - 1, sum_step, 0)

    def last_copy(i):
        return remote(fs.at[i], fr.at[i], f_s.at[i], f_r.at[i], (mate_y, across, mate_x)[i])

    sum_b(z, other_y)
    fs[0] = acc_b[:, :tail].astype(jnp.bfloat16)
    fs[1] = acc_b[:, tail:].astype(jnp.bfloat16)
    last_copy(0).start()
    last_copy(1).start()
    sum_b(z, e)
    fs[2] = acc_b[:, tail:].astype(jnp.bfloat16)
    last_copy(2).start()
    sum_a(z, e)

    def place(low, value):
        for q in range(2):
            start, stop = max(low, q * quarter), min(low + value.shape[1], (q + 1) * quarter)
            if start < stop:
                fin[q, :, start - q * quarter : stop - q * quarter] = value[:, start - low : stop - low]

    place(0, acc_a[...])
    for i in range(3):
        last_copy(i).wait_recv()
    place(
        keep,
        acc_b[:, :tail] + fr[0].astype(jnp.float32) + fr[1].astype(jnp.float32) + fr[2].astype(jnp.float32),
    )
    swap = remote(fin.at[1 - c], fin_in, o_s, o_r, mate_c)
    swap.start()
    out_ref[rows_of(c), :] = (fin[c] + sh_out[c]).astype(jnp.bfloat16)
    swap.wait_recv()
    out_ref[rows_of(1 - c), :] = (fin_in[...] + sh_out[1 - c]).astype(jnp.bfloat16)

    swap.wait_send()
    for i in range(3):
        last_copy(i).wait_send()
        weight_copy(i, c).wait_send()
    y_first().wait_send()
    for k in range(1, n):
        wt_copy(k, lax.rem(e + k, n)).wait_send()
    for k in range(1, tp_count):
        sh_copy(k, t, lax.rem(t + k, tp_count)).wait_send()

    def drain(i, carry):
        p, g = slot_group(i)

        def sent(line, s_up, s_down):
            @pl.when(ups(p))
            def _():
                line(g, s_up, z_up).wait_send()

            @pl.when(downs(p))
            def _():
                line(g, s_down, z_down).wait_send()

        sent(line_b, bu_s, bd_s)

        @pl.when(i % 2 == 0)
        def _():
            sent(line_a, au_s, ad_s)
            y_copy(g).wait_send()

            @pl.when(p != z)
            def _():
                rza_copy(p, 0, z_up).wait_send()

        @pl.when(i % 2 == 1)
        def _():
            ry_copy(p).wait_send()

        @pl.when(i > 0)
        def _():
            x_copy(g).wait_send()

        rx_copy(g).wait_send()

        @pl.when(p != z)
        def _():
            rzb_copy(g, 0, z_up).wait_send()

        return carry

    lax.fori_loop(0, n, drain, 0)


def dense_exchange(
    tokens, norm_gain, expert_ids, route_weights, expert_gate, expert_up, expert_down,
    shared_gate, shared_up, shared_down,
):
    n = lax.axis_size("ep")
    tp_count = lax.axis_size("tp")
    minor = 1 << (n.bit_length() - 1) // 2
    major = n // minor
    rows, width = tokens.shape
    half = rows // 2
    side = width // 2
    quarter = width // tp_count
    near = side * NEAR // 8 // LANES * LANES
    keep = side * KEEP // 8 // LANES * LANES
    tail = side - keep
    ff = expert_gate.shape[2]
    share = shared_gate.shape[1]
    bf16, f32 = jnp.bfloat16, jnp.float32
    dma = pltpu.SemaphoreType.DMA
    vmem = pl.BlockSpec(memory_space=pltpu.VMEM)
    anywhere = pl.BlockSpec(memory_space=pl.ANY)
    return pl.pallas_call(
        functools.partial(dense_kernel, n, tp_count, minor, near, keep, LAG, TURN),
        out_shape=jax.ShapeDtypeStruct((rows, quarter), bf16),
        in_specs=[vmem] * 3 + [anywhere] * 7,
        out_specs=vmem,
        scratch_shapes=[
            pltpu.VMEM((2, half, width), bf16),
            pltpu.VMEM((n, half, width), bf16),
            pltpu.VMEM((half, width), bf16),
            pltpu.VMEM((n, 1, rows), f32),
            pltpu.VMEM((n, 1, rows), f32),
            pltpu.VMEM((2, width, ff), bf16),
            pltpu.VMEM((2, width, ff), bf16),
            pltpu.VMEM((2, ff, width), bf16),
            pltpu.VMEM((width, share), bf16),
            pltpu.VMEM((width, share), bf16),
            pltpu.VMEM((share * tp_count, quarter), bf16),
            pltpu.VMEM((tp_count, 2, half, share), bf16),
            pltpu.VMEM((2, half, quarter), f32),
            pltpu.VMEM((n, half, keep), f32),
            pltpu.VMEM((n, half, 2 * tail), f32),
            pltpu.VMEM((n, half, keep), bf16),
            pltpu.VMEM((n, half, keep), bf16),
            pltpu.VMEM((major, half, keep), bf16),
            pltpu.VMEM((major, half, keep), bf16),
            pltpu.VMEM((major, half, keep), bf16),
            pltpu.VMEM((2, major, half, keep), bf16),
            pltpu.VMEM((n, half, 2 * tail), bf16),
            pltpu.VMEM((2, n, half, 2 * tail), bf16),
            pltpu.VMEM((3, half, tail), bf16),
            pltpu.VMEM((3, half, tail), bf16),
            pltpu.VMEM((2, half, quarter), f32),
            pltpu.VMEM((half, quarter), f32),
            pltpu.VMEM((half, keep), f32),
            pltpu.VMEM((half, 2 * tail), f32),
            dma((9,)), dma((n,)), dma((n,)), dma((3,)), dma((3,)), dma((tp_count,)), dma((tp_count,)), dma,
            dma((n,)), dma((n,)), dma((n,)), dma((n,)), dma((n,)), dma((n,)),
            dma((n,)), dma((n,)), dma((n,)), dma((n,)),
            dma((n,)), dma((n,)), dma((major,)), dma((major,)),
            dma((major,)), dma((2, major)), dma((n,)), dma((2, n)), dma((3,)), dma((3,)), dma, dma,
        ],
        compiler_params=pltpu.CompilerParams(
            collective_id=0, has_side_effects=True, vmem_limit_bytes=60 << 20
        ),
        name="dense_moe",
    )(
        expert_ids.T, route_weights.T, norm_gain.reshape(1, width), tokens,
        expert_gate[0], expert_up[0], expert_down[0],
        shared_gate, shared_up, shared_down,
    )


def local(tokens, *rest):
    ep_count = lax.axis_size("ep")
    pair_count = lax.axis_size("tp") // 2
    dense_bytes = 4 * ep_count * tokens.size * tokens.dtype.itemsize
    minor = 1 << (ep_count.bit_length() - 1) // 2
    if pair_count == 2 and minor == 2 and dense_bytes <= 24 << 20:
        return dense_exchange(tokens, *rest)
    return routed_exchange(tokens, *rest)


def solution(mesh):
    return jax.shard_map(
        local,
        mesh=mesh,
        in_specs=(
            P("ep", None),
            P(),
            P("ep", None),
            P("ep", None),
            P(("ep", "tp"), None, None),
            P(("ep", "tp"), None, None),
            P(("ep", "tp"), None, None),
            P(None, "tp"),
            P(None, "tp"),
            P(None, "tp"),
        ),
        out_specs=P("ep", "tp"),
        check_vma=False,
    )
```

time: 84.2 us -> 69.5 us (0.83)
  Pallas kernels: 80.5 us -> 67.7 us
  other arithmetic: 1.3 us -> 0 us
    pallas_call x1, Pallas kernels: 80.5 us -> 67.7 us  [dense_exchange(): pl.pallas_call(functools.partial(dense_kernel, n, tp_count, minor, near,...]
    reduce_sum x1 -> x0, other arithmetic: 1.3 us -> none  [dense_exchange(): jnp.sum(jnp.where(expert_ids[None, :, :] == expert_iota[:, None, None], r...]
    unnamed x3 -> x1, local copies, waits for them, and re-layouts: 2.25 us -> 1.57 us
where the time goes in v1:
time: 69.5 us; the launch traced here: 69.3 us
  Pallas kernels  67.7 us (97%)
  local copies, waits for them, and re-layouts  1.57 us (2%)
    pallas_call x1, Pallas kernels, dense_exchange(): pl.pallas_call(functools.partial(dense_kernel, n, tp_count, minor, near,...  67.7 us
    unnamed x1, local copies, waits for them, and re-layouts  1.57 us

profile of v1, /device:TPU:0, one launch (start us, length us, event | category | flops | bytes accessed | tf_op | source)
XLA Modules:
  0.0 69.3 jit_solution(13074605413045284551)
XLA Ops:
  0.0 67.7 %dense_moe.1 = bf16[128,512]{1,0:T(8,128)(2,1)} custom-call(s32[6,128]{1,0:T(8,128)} %bitcast.10, f32[6,128]{1,0:T(8,128)} %bitcast.11, f32[1,2048]{1,0:T(1,128)} %bitcast.9, bf16[128,2048]{1,0:T(8,128)(2,1)} %tok_hbm.1, bf16[2048,256]{1,0:T(8,128)(2,1)} %bitcast.6, bf16[2048,256]{1,0:T(8,128)(2,1)} %bitcast.7, bf16[256,2048]{1,0:T(8,128)(2,1)} %bitcast.8, ...), custom_call_target="tpu_custom_call" | custom-call | tf_op jit(solution)/shard_map/dense_moe/pallas_call | solution.py:590
  67.7 1.6 %copy.12 = bf16[128,512]{1,0:T(8,128)(2,1)} copy(bf16[128,512]{1,0:T(8,128)(2,1)} %dense_moe.1) | data formatting | bytes 262144

commit v2 on v1

--- a/solution.py
+++ b/solution.py
@@ -115,32 +115,50 @@
 
 MESH = pl.DeviceIdType.MESH
 LANES = 128
-KEEP = 6
-NEAR = 6
-TURN = 2
-LAG = 2
+BOTH_KEEP = 2
+KEEP = 4
+WIDE = 2
+NEAR = 4
 
 
 def silu(v):
     return v / (1.0 + jnp.exp(-v))
 
 
+KINDS = ("a", "c", "b", "x", "k", "t", "r", "s", "zb", "zc", "za")
+OUTER = [
+    ("b", 1), ("a", 2), ("x", 1), ("c", 2), ("b", 2), ("k", 0), ("b", 3), ("x", 3), ("a", 4), ("c", 4), ("k", 1, 2), ("b", 4), ("b", 5),
+    ("x", 5), ("a", 6), ("c", 6), ("k", 3, 4), ("b", 6), ("zb", 0), ("b", 7), ("x", 7), ("k", 5, 6), ("zb", 1), ("r", 3), ("zc", 0),
+    ("za", 0), ("s", 0), ("k", 7), ("zb", 2), ("t", 0), ("t", 1), ("zc", 1), ("zc", 2), ("r", 5), ("za", 1), ("r", 7), ("za", 2), ("r", 1),
+]
+INNER = [
+    ("b", 1), ("a", 2), ("a", 4), ("x", 1), ("c", 2), ("c", 4), ("b", 2), ("b", 4), ("b", 3), ("b", 5), ("k", 0), ("x", 3), ("x", 5), ("a", 6),
+    ("k", 2, 4), ("c", 6), ("b", 6), ("b", 7), ("k", 1, 3), ("x", 7), ("k", 5, 6), ("k", 7), ("t", 0), ("t", 1), ("s", 0),
+    ("r", 3), ("r", 5), ("zb", 0), ("zc", 0), ("r", 7), ("za", 0), ("zb", 1), ("zc", 1), ("za", 1), ("r", 1), ("zb", 2), ("zc", 2), ("za", 2),
+]
+
+
+def plans_for(n):
+    return OUTER, INNER
+
+
 def dense_kernel(
-    ep_count, tp_count, minor, near, keep, lag, turn,
-    ids_ref, rw_ref, gain_ref, tok_hbm, gate_hbm, up_hbm, down_hbm, sg_hbm, su_hbm, sd_hbm,
+    ep_count, tp_count, minor, near, wide, keep, both_keep, plans,
+    ids_hbm, rw_hbm, gain_hbm, tok_hbm, gate_hbm, up_hbm, down_hbm, sg_hbm, su_hbm, sd_hbm,
     out_ref,
-    tok, xb, xo, wtab, wr, wg, wu, wd, sg, su, sd, sh_all, sh_out,
-    pa, pb, xs, xr, ys, yr, zas, zar, zbs, zbr, fs, fr, fin, fin_in, acc_a, acc_b,
+    ids_ref, rw_ref, gain_ref, tok, xb, xo, wtab, wr, wg, wu, wd, sg, su, sd, sh_all, sh_out,
+    pa, pb, pc, xs, xr, ys, yr, ycs, ycr, zas, zar, zbs, zbr, zcs, zcr, fs, fr, gs, gr, fin, fin_in, acc_a, acc_b, acc_c,
     load_sem, wt_s, wt_r, we_s, we_r, sh_s, sh_r, yb_s,
-    au_s, ad_s, a_r, bu_s, bd_s, b_r, ya_s, ya_r, xa_s, xa_r,
-    rx_s, rx_r, ry_s, ry_r, rza_s, rza_r, rzb_s, rzb_r, f_s, f_r, o_s, o_r,
+    au_s, ad_s, a_r, bu_s, bd_s, b_r, cu_s, cd_s, c_r, ya_s, ya_r, yc_s, yc_r, xa_s, xa_r,
+    rx_s, rx_r, ry_s, ry_r, ryc_s, ryc_r, rza_s, rza_r, rzb_s, rzb_r, rzc_s, rzc_r, f_s, f_r, g_s, g_r, o_s, o_r,
 ):
     n = ep_count
     major = n // minor
     half, width = xo.shape
     side = width // 2
     quarter = width // tp_count
-    tail = side - keep
+    tail = side - keep - both_keep
+    middle = keep + both_keep
     e = lax.axis_index("ep")
     t = lax.axis_index("tp")
     z = e // minor
@@ -155,6 +173,7 @@
     across = {"ep": other_y, "tp": t2}
     z_up = {"ep": lax.rem(e + minor, n)}
     z_down = {"ep": lax.rem(e + n - minor, n)}
+    far = {"ep": (major - 1 - z) * minor + y}
     is_end = (z == 0) | (z == major - 1)
 
     barrier = pltpu.get_barrier_semaphore()
@@ -188,11 +207,14 @@
                 (sg_hbm, sg),
                 (su_hbm, su),
                 (sd_hbm, sd),
+                (gain_hbm, gain_ref),
+                (ids_hbm, ids_ref),
+                (rw_hbm, rw_ref),
             )
         )
     ]
-    for load in loads:
-        load.start()
+    for i in (0, 9, 10, 11, 2, 3, 4, 5, 1, 6, 7, 8):
+        loads[i].start()
 
     step = 16
 
@@ -219,7 +241,10 @@
         return row
 
     loads[0].wait()
+    loads[9].wait()
     norm_into(0, store_own)
+    loads[10].wait()
+    loads[11].wait()
     for d in range(n):
         wtab[d] = weights_for(d * (tp_count // 2) + xi)
     wr[e] = weights_for(e * (tp_count // 2) + xi)
@@ -227,7 +252,8 @@
 
     mine = pl.ds(pl.multiple_of(xi * near, LANES), near)
     theirs = pl.ds(pl.multiple_of((1 - xi) * near, LANES), near)
-    rest = pl.ds(2 * near, width - 2 * near)
+    shared_cols = pl.ds(2 * near, wide)
+    rest = pl.ds(2 * near + wide, width - 2 * near - wide)
 
     def line_a(g, s, who):
         ref = xb.at[g, :, mine]
@@ -237,6 +263,14 @@
         ref = xb.at[g, :, rest]
         return remote(ref, ref, s.at[g], b_r.at[g], who)
 
+    def line_c(g, s, who):
+        ref = xb.at[g, :, shared_cols]
+        return remote(ref, ref, s.at[g], c_r.at[g], who)
+
+    def y_shared(g):
+        ref = xb.at[g, :, shared_cols]
+        return remote(ref, ref, yc_s.at[g], yc_r.at[g], mate_y)
+
     def y_first():
         ref = xb.at[e, :, rest]
         return remote(ref, ref, yb_s, b_r.at[e], mate_y)
@@ -269,7 +303,7 @@
     def order(j):
         k = jnp.minimum(z, major - 1 - z)
         d = (j + 1) // 2
-        close = jnp.where(j % 2 == 1, z - d, z + d)
+        close = jnp.where((j % 2 == 1) == (2 * z < major), z - d, z + d)
         far = jnp.where(z <= major - 1 - z, j, major - 1 - j)
         return jnp.where(j <= 2 * k, close, far)
 
@@ -295,7 +329,9 @@
 
     forward(z, e, line_a, au_s, ad_s)
     y_first().start()
+    forward(z, e, line_c, cu_s, cd_s)
     y_copy(e).start()
+    y_shared(e).start()
     forward(z, e, line_b, bu_s, bd_s)
     for k in range(1, n):
         wt_copy(k, lax.rem(e + k, n)).start()
@@ -327,6 +363,12 @@
     def ry_copy(p):
         return remote(ys.at[p], yr.at[p], ry_s.at[p], ry_r.at[p], mate_y)
 
+    def ryc_copy(p):
+        return remote(ycs.at[p], ycr.at[p], ryc_s.at[p], ryc_r.at[p], mate_y)
+
+    def rzc_copy(p, lane, who):
+        return remote(zcs.at[p], zcr.at[lane, p], rzc_s.at[p], rzc_r.at[lane, p], who)
+
     def rza_copy(p, lane, who):
         return remote(zas.at[p], zar.at[lane, p], rza_s.at[p], rza_r.at[lane, p], who)
 
@@ -337,9 +379,13 @@
         lax.broadcasted_iota(jnp.int32, (half, 2 * half), 0) + c * half
     )
 
-    def compute(g):
-        weight = jnp.sum(jnp.where(diagonal, wr[g], 0.0), axis=1, keepdims=True)
-        x = xb[g]
+    def weight_of(g):
+        return jnp.sum(jnp.where(diagonal, wr[g], 0.0), axis=1, keepdims=True)
+
+    def compute(i, j, first, second, both):
+        pair = ((i, first), (j, second))
+        weight = jnp.concatenate([weight_of(first), weight_of(second)], axis=0)
+        x = jnp.concatenate([xb[first], xb[second]], axis=0)
         acts = []
         for h in range(2):
             g_sum = jnp.dot(x, wg[h], preferred_element_type=jnp.float32)
@@ -351,139 +397,222 @@
             total += jnp.dot(acts[1], wd[1, :, low:high], preferred_element_type=jnp.float32)
             return total * weight
 
-        xs[g] = columns(side, side + keep).astype(jnp.bfloat16)
-        rx_copy(g).start()
-        pa[g] = columns(0, keep)
-        pb[g, :, :tail] = columns(keep, side)
-        pb[g, :, tail:] = columns(side + keep, width)
+        sent = columns(side, side + keep).astype(jnp.bfloat16)
+        kept = columns(0, keep)
+        kept_c = columns(keep, middle)
+        rest_c = columns(side + keep, side + middle)
+        main = columns(middle, side)
+        rest = columns(side + middle, width)
+
+        def put(k):
+            index, g = pair[k]
+            part = slice(k * half, (k + 1) * half)
+            xs[g] = sent[part]
+
+            @pl.when(index > 1)
+            def _():
+                rx_copy(g).start()
+
+            pc[g, :, :both_keep] = kept_c[part]
+            pc[g, :, both_keep:] = rest_c[part]
+
+            @pl.when(index % 2 == 1)
+            def _():
+                p = g // minor
+                ycs[p] = pc[g].astype(jnp.bfloat16)
+                ryc_copy(p).start()
+
+            pa[g] = kept[part]
+            pb[g, :, :tail] = main[part]
+            pb[g, :, tail:] = rest[part]
+
+        put(0)
+
+        @pl.when(both)
+        def _():
+            put(1)
+
+    def add_lanes(p, acc, copy, key, received, direct):
+        below = downs(p)
+        above = ups(p)
+        if direct:
+            below &= jnp.logical_not((p == major - 1) & (z == 1))
+            above &= jnp.logical_not((p == 0) & (z == major - 2))
+
+        @pl.when(below)
+        def _():
+            copy(key, 0, z_up).wait_recv()
+            acc[...] += received[0, key].astype(jnp.float32)
+
+        @pl.when(above)
+        def _():
+            copy(key, 1, z_up).wait_recv()
+            acc[...] += received[1, key].astype(jnp.float32)
+
+        if direct:
+
+            @pl.when((p == z) & is_end)
+            def _():
+                copy(key, 2, far).wait_recv()
+                acc[...] += received[2, key].astype(jnp.float32)
 
     def sum_b(p, g):
         acc_b[...] = pb[g]
-
-        @pl.when(downs(p))
-        def _():
-            rzb_copy(g, 0, z_up).wait_recv()
-            acc_b[...] += zbr[0, g].astype(jnp.float32)
-
-        @pl.when(ups(p))
-        def _():
-            rzb_copy(g, 1, z_up).wait_recv()
-            acc_b[...] += zbr[1, g].astype(jnp.float32)
+        add_lanes(p, acc_b, rzb_copy, g, zbr, False)
+
+    def sum_c(p, g):
+        ryc_copy(p).wait_recv()
+        acc_c[...] = pc[g] + ycr[p].astype(jnp.float32)
+        add_lanes(p, acc_c, rzc_copy, p, zcr, True)
 
     def sum_a(p, g):
         rx_copy(g).wait_recv()
         ry_copy(p).wait_recv()
         acc_a[...] = pa[g] + xr[g].astype(jnp.float32) + yr[p].astype(jnp.float32)
-
-        @pl.when(downs(p))
-        def _():
-            rza_copy(p, 0, z_up).wait_recv()
-            acc_a[...] += zar[0, p].astype(jnp.float32)
-
-        @pl.when(ups(p))
-        def _():
-            rza_copy(p, 1, z_up).wait_recv()
-            acc_a[...] += zar[1, p].astype(jnp.float32)
-
-    def line_sums(p):
-        def send(copy, key):
-            @pl.when(p > z)
+        add_lanes(p, acc_a, rza_copy, p, zar, True)
+
+    def line_order(q):
+        above = major - 1 - z
+        low = jnp.where(q < above, z + 1 + q, z - 1 - (q - above))
+        high = jnp.where(q < z, z - 1 - q, z + 1 + (q - z))
+        return jnp.where(2 * z < major, low, high)
+
+    def send_sum(copy, key, p, direct):
+        whole = is_end & (p == major - 1 - z)
+        step_by = jnp.logical_not(whole) if direct else p != z
+
+        @pl.when((p > z) & step_by)
+        def _():
+            copy(key, 0, z_up).start()
+
+        @pl.when((p < z) & step_by)
+        def _():
+            copy(key, 1, z_down).start()
+
+        if direct:
+
+            @pl.when(whole)
             def _():
-                copy(key, 0, z_up).start()
-
-            @pl.when(p < z)
+                copy(key, 2, far).start()
+
+    def do_a(i):
+        p, g = slot_group(i)
+        line_a(g, au_s, z_up).wait_recv()
+        forward(p, g, line_a, au_s, ad_s)
+        y_copy(g).start()
+        x_copy(g).start()
+
+    def do_c(i):
+        p, g = slot_group(i)
+        line_c(g, cu_s, z_up).wait_recv()
+        forward(p, g, line_c, cu_s, cd_s)
+        y_shared(g).start()
+
+    def do_b(i):
+        p, g = slot_group(i)
+        line_b(g, bu_s, z_up).wait_recv()
+        forward(p, g, line_b, bu_s, bd_s)
+
+    def do_x(i):
+        _, g = slot_group(i)
+        y_copy(g).wait_recv()
+        x_copy(g).start()
+
+    def do_k(code):
+        i, j = code // (n + 1), code % (n + 1)
+        both = j < n
+        _, first = slot_group(i)
+        _, second = slot_group(jnp.where(both, j, i))
+
+        @pl.when(i == 0)
+        def _():
+            for k in range(3):
+                weight_copy(k, 1 - c).wait_recv()
+
+        def ready(index, g):
+            @pl.when(index % 2 == 1)
             def _():
-                copy(key, 1, z_down).start()
-
+                y_shared(g).wait_recv()
+
+            x_arrival(g).wait_recv()
+            wt_arrival(g).wait_recv()
+
+        @pl.when(i > 0)
+        def _():
+            ready(i, first)
+
+        @pl.when(both)
+        def _():
+            ready(j, second)
+
+        compute(i, j, first, second, both)
+
+    def do_t(i):
+        _, g = slot_group(i)
+        rx_copy(g).start()
+
+    def do_r(i):
+        p, g = slot_group(i)
+        rx_copy(g).wait_recv()
+        ys[p] = (pa[g] + xr[g].astype(jnp.float32)).astype(jnp.bfloat16)
+        ry_copy(p).start()
+
+    def do_s(_):
+        loads[8].wait()
+        for k in range(1, tp_count):
+            sh_copy(k, lax.rem(t + tp_count - k, tp_count), t).wait_recv()
+        share = sg.shape[1]
+        for r in range(2):
+            shared = jnp.zeros((half, quarter), jnp.float32)
+            for q in range(tp_count):
+                shared += jnp.dot(
+                    sh_all[q, r], sd[q * share : (q + 1) * share, :],
+                    preferred_element_type=jnp.float32,
+                )
+            sh_out[r] = shared
+
+    def do_zb(q):
+        p = line_order(q)
         for yy in (1 - y, y):
             g = p * minor + yy
             sum_b(p, g)
             zbs[g] = acc_b[...].astype(jnp.bfloat16)
-            send(rzb_copy, g)
+            send_sum(rzb_copy, g, p, False)
+
+    def do_zc(q):
+        p = line_order(q)
+        sum_c(p, p * minor + y)
+        zcs[p] = acc_c[...].astype(jnp.bfloat16)
+        send_sum(rzc_copy, p, p, True)
+
+    def do_za(q):
+        p = line_order(q)
         sum_a(p, p * minor + y)
         zas[p] = acc_a[...].astype(jnp.bfloat16)
-        send(rza_copy, p)
+        send_sum(rza_copy, p, p, True)
+
+    actions = (do_a, do_c, do_b, do_x, do_k, do_t, do_r, do_s, do_zb, do_zc, do_za)
 
     def main_step(i, carry):
-        @pl.when((i >= 1) & (i < n))
-        def _():
-            p, g = slot_group(i)
-
-            @pl.when(i % 2 == 0)
-            def _():
-                line_a(g, au_s, z_up).wait_recv()
-                forward(p, g, line_a, au_s, ad_s)
-                y_copy(g).start()
-                x_copy(g).start()
-
-            line_b(g, bu_s, z_up).wait_recv()
-            forward(p, g, line_b, bu_s, bd_s)
-
-        @pl.when((i >= 2) & (i <= n) & (i % 2 == 0))
-        def _():
-            _, g = slot_group(i - 1)
-            y_copy(g).wait_recv()
-            x_copy(g).start()
-
-        @pl.when(i == lag)
-        def _():
-            for j in range(3):
-                weight_copy(j, 1 - c).wait_recv()
-
-        @pl.when((i >= lag) & (i < n + lag))
-        def _():
-            _, g = slot_group(i - lag)
-
-            @pl.when(i > lag)
-            def _():
-                x_arrival(g).wait_recv()
-                wt_arrival(g).wait_recv()
-
-            compute(g)
-
-        @pl.when(i == n)
-        def _():
-            loads[8].wait()
-            for k in range(1, tp_count):
-                sh_copy(k, lax.rem(t + tp_count - k, tp_count), t).wait_recv()
-            share = sg.shape[1]
-            for r in range(2):
-                shared = jnp.zeros((half, quarter), jnp.float32)
-                for q in range(tp_count):
-                    shared += jnp.dot(
-                        sh_all[q, r], sd[q * share : (q + 1) * share, :],
-                        preferred_element_type=jnp.float32,
-                    )
-                sh_out[r] = shared
-
-        @pl.when((i >= lag + turn + 1) & (i < n + lag + turn) & ((i - lag - turn) % 2 == 1))
-        def _():
-            p, g = slot_group(i - lag - turn)
-            rx_copy(g).wait_recv()
-            ys[p] = (pa[g] + xr[g].astype(jnp.float32)).astype(jnp.bfloat16)
-            ry_copy(p).start()
-
-        @pl.when(is_end & (i >= lag + turn + 4) & ((i - lag - turn) % 2 == 0))
-        def _():
-            line_sums(order((i - lag - turn - 2) // 2))
+        for a, action in enumerate(actions):
+            outer, inner = (
+                sum((jnp.where(i == k, slot[a] + 1, 0) for k, slot in enumerate(plan) if slot[a] is not None), i * 0)
+                for plan in plans
+            )
+            code = jnp.where(is_end, outer, inner)
+
+            @pl.when(code > 0)
+            def _(action=action, code=code):
+                action(code - 1)
 
         return carry
 
-    lax.fori_loop(0, n + lag + turn + 1, main_step, 0)
-
-    @pl.when(jnp.logical_not(is_end))
-    def _():
-        def sum_step(q, carry):
-            above = major - 1 - z
-            low = jnp.where(q < above, z + 1 + q, z - 1 - (q - above))
-            high = jnp.where(q < z, z - 1 - q, z + 1 + (q - z))
-            line_sums(jnp.where(2 * z < major, low, high))
-            return carry
-
-        lax.fori_loop(0, major - 1, sum_step, 0)
+    lax.fori_loop(0, max(len(plan) for plan in plans), main_step, 0)
 
     def last_copy(i):
         return remote(fs.at[i], fr.at[i], f_s.at[i], f_r.at[i], (mate_y, across, mate_x)[i])
+
+    last_c = remote(gs, gr, g_s, g_r, mate_x)
 
     sum_b(z, other_y)
     fs[0] = acc_b[:, :tail].astype(jnp.bfloat16)
@@ -493,6 +622,9 @@
     sum_b(z, e)
     fs[2] = acc_b[:, tail:].astype(jnp.bfloat16)
     last_copy(2).start()
+    sum_c(z, e)
+    gs[...] = acc_c[:, both_keep:].astype(jnp.bfloat16)
+    last_c.start()
     sum_a(z, e)
 
     def place(low, value):
@@ -502,10 +634,12 @@
                 fin[q, :, start - q * quarter : stop - q * quarter] = value[:, start - low : stop - low]
 
     place(0, acc_a[...])
+    last_c.wait_recv()
+    place(keep, acc_c[:, :both_keep] + gr[...].astype(jnp.float32))
     for i in range(3):
         last_copy(i).wait_recv()
     place(
-        keep,
+        middle,
         acc_b[:, :tail] + fr[0].astype(jnp.float32) + fr[1].astype(jnp.float32) + fr[2].astype(jnp.float32),
     )
     swap = remote(fin.at[1 - c], fin_in, o_s, o_r, mate_c)
@@ -515,6 +649,7 @@
     out_ref[rows_of(1 - c), :] = (fin_in[...] + sh_out[1 - c]).astype(jnp.bfloat16)
 
     swap.wait_send()
+    last_c.wait_send()
     for i in range(3):
         last_copy(i).wait_send()
         weight_copy(i, c).wait_send()
@@ -541,15 +676,19 @@
         @pl.when(i % 2 == 0)
         def _():
             sent(line_a, au_s, ad_s)
+            sent(line_c, cu_s, cd_s)
             y_copy(g).wait_send()
+            y_shared(g).wait_send()
 
             @pl.when(p != z)
             def _():
                 rza_copy(p, 0, z_up).wait_send()
+                rzc_copy(p, 0, z_up).wait_send()
 
         @pl.when(i % 2 == 1)
         def _():
             ry_copy(p).wait_send()
+            ryc_copy(p).wait_send()
 
         @pl.when(i > 0)
         def _():
@@ -564,6 +703,17 @@
         return carry
 
     lax.fori_loop(0, n, drain, 0)
+
+
+def slots_of(listing, n):
+    slots, last = [], len(KINDS)
+    for kind, *args in listing:
+        a = KINDS.index(kind)
+        if a <= last and (a == last or last == len(KINDS) or a < last):
+            slots.append([None] * len(KINDS))
+        slots[-1][a] = args[0] * (n + 1) + (args[1] if len(args) > 1 else n) if kind == "k" else args[0]
+        last = a
+    return slots
 
 
 def dense_exchange(
@@ -579,8 +729,10 @@
     side = width // 2
     quarter = width // tp_count
     near = side * NEAR // 8 // LANES * LANES
+    wide = 2 * (side * WIDE // 8 // LANES * LANES)
     keep = side * KEEP // 8 // LANES * LANES
-    tail = side - keep
+    both_keep = side * BOTH_KEEP // 8 // LANES * LANES
+    tail = side - keep - both_keep
     ff = expert_gate.shape[2]
     share = shared_gate.shape[1]
     bf16, f32 = jnp.bfloat16, jnp.float32
@@ -588,11 +740,14 @@
     vmem = pl.BlockSpec(memory_space=pltpu.VMEM)
     anywhere = pl.BlockSpec(memory_space=pl.ANY)
     return pl.pallas_call(
-        functools.partial(dense_kernel, n, tp_count, minor, near, keep, LAG, TURN),
-        out_shape=jax.ShapeDtypeStruct((rows, quarter), bf16),
-        in_specs=[vmem] * 3 + [anywhere] * 7,
+        functools.partial(dense_kernel, n, tp_count, minor, near, wide, keep, both_keep, [slots_of(p, n) for p in plans_for(n)]),
+        out_shape=pltpu.VMEM((rows, quarter), bf16),
+        in_specs=[anywhere] * 10,
         out_specs=vmem,
         scratch_shapes=[
+            pltpu.VMEM((expert_ids.shape[1], rows), jnp.int32),
+            pltpu.VMEM((expert_ids.shape[1], rows), f32),
+            pltpu.VMEM((1, width), f32),
             pltpu.VMEM((2, half, width), bf16),
             pltpu.VMEM((n, half, width), bf16),
             pltpu.VMEM((half, width), bf16),
@@ -608,25 +763,34 @@
             pltpu.VMEM((2, half, quarter), f32),
             pltpu.VMEM((n, half, keep), f32),
             pltpu.VMEM((n, half, 2 * tail), f32),
+            pltpu.VMEM((n, half, 2 * both_keep), f32),
             pltpu.VMEM((n, half, keep), bf16),
             pltpu.VMEM((n, half, keep), bf16),
             pltpu.VMEM((major, half, keep), bf16),
             pltpu.VMEM((major, half, keep), bf16),
+            pltpu.VMEM((major, half, 2 * both_keep), bf16),
+            pltpu.VMEM((major, half, 2 * both_keep), bf16),
             pltpu.VMEM((major, half, keep), bf16),
-            pltpu.VMEM((2, major, half, keep), bf16),
+            pltpu.VMEM((3, major, half, keep), bf16),
             pltpu.VMEM((n, half, 2 * tail), bf16),
             pltpu.VMEM((2, n, half, 2 * tail), bf16),
+            pltpu.VMEM((major, half, 2 * both_keep), bf16),
+            pltpu.VMEM((3, major, half, 2 * both_keep), bf16),
             pltpu.VMEM((3, half, tail), bf16),
             pltpu.VMEM((3, half, tail), bf16),
+            pltpu.VMEM((half, both_keep), bf16),
+            pltpu.VMEM((half, both_keep), bf16),
             pltpu.VMEM((2, half, quarter), f32),
             pltpu.VMEM((half, quarter), f32),
             pltpu.VMEM((half, keep), f32),
             pltpu.VMEM((half, 2 * tail), f32),
-            dma((9,)), dma((n,)), dma((n,)), dma((3,)), dma((3,)), dma((tp_count,)), dma((tp_count,)), dma,
+            pltpu.VMEM((half, 2 * both_keep), f32),
+            dma((12,)), dma((n,)), dma((n,)), dma((3,)), dma((3,)), dma((tp_count,)), dma((tp_count,)), dma,
+            dma((n,)), dma((n,)), dma((n,)), dma((n,)), dma((n,)), dma((n,)), dma((n,)), dma((n,)), dma((n,)),
             dma((n,)), dma((n,)), dma((n,)), dma((n,)), dma((n,)), dma((n,)),
-            dma((n,)), dma((n,)), dma((n,)), dma((n,)),
-            dma((n,)), dma((n,)), dma((major,)), dma((major,)),
-            dma((major,)), dma((2, major)), dma((n,)), dma((2, n)), dma((3,)), dma((3,)), dma, dma,
+            dma((n,)), dma((n,)), dma((major,)), dma((major,)), dma((major,)), dma((major,)),
+            dma((major,)), dma((3, major)), dma((n,)), dma((2, n)), dma((major,)), dma((3, major)),
+            dma((3,)), dma((3,)), dma, dma, dma, dma,
         ],
         compiler_params=pltpu.CompilerParams(
             collective_id=0, has_side_effects=True, vmem_limit_bytes=60 << 20

time: 69.5 us -> 59.8 us (0.86)
  Pallas kernels: 67.7 us -> 59 us
  local copies, waits for them, and re-layouts: 1.57 us -> 0.66 us
    pallas_call x1, Pallas kernels: 67.7 us -> 59 us  [dense_exchange(): pl.pallas_call(functools.partial(dense_kernel, n, tp_count, minor, near,...]
    unnamed x1, local copies, waits for them, and re-layouts: 1.57 us -> 0.66 us
where the time goes in v2:
time: 59.8 us; the launch traced here: 59.7 us
  Pallas kernels  59 us (99%)
  local copies, waits for them, and re-layouts  0.66 us (1%)
    pallas_call x1, Pallas kernels, dense_exchange(): pl.pallas_call(functools.partial(dense_kernel, n, tp_count, minor, near,...  59 us

profile of v2, /device:TPU:0, one launch (start us, length us, event | category | flops | bytes accessed | tf_op | source)
XLA Modules:
  0.0 59.7 jit_solution(14392328525657105532)
XLA Ops:
  0.0 59.0 %dense_moe.1 = bf16[128,512]{1,0:T(8,128)(2,1)S(1)} custom-call(s32[6,128]{1,0:T(8,128)} %bitcast.10, f32[6,128]{1,0:T(8,128)} %bitcast.11, f32[1,2048]{1,0:T(1,128)} %bitcast.9, bf16[128,2048]{1,0:T(8,128)(2,1)} %tok_hbm.1, bf16[2048,256]{1,0:T(8,128)(2,1)} %bitcast.6, bf16[2048,256]{1,0:T(8,128)(2,1)} %bitcast.7, bf16[256,2048]{1,0:T(8,128)(2,1)} %bitcast.8, ...), custom_call_target="tpu_custom_call" | custom-call | tf_op jit(solution)/shard_map/dense_moe/pallas_call | solution.py:742
  59.0 0.7 %copy.12 = bf16[128,512]{1,0:T(8,128)(2,1)} copy(bf16[128,512]{1,0:T(8,128)(2,1)S(1)} %dense_moe.1) | data formatting | bytes 262144

commit v3 on v2

--- a/solution.py
+++ b/solution.py
@@ -115,31 +115,34 @@
 
 MESH = pl.DeviceIdType.MESH
 LANES = 128
-BOTH_KEEP = 2
+BOTH_KEEP = 3
 KEEP = 4
-WIDE = 2
-NEAR = 4
+WIDE = 3
+NEAR = 3
 
 
 def silu(v):
     return v / (1.0 + jnp.exp(-v))
 
 
-KINDS = ("a", "c", "b", "x", "k", "t", "r", "s", "zb", "zc", "za")
+FIELD = 16
+KINDS = ("a", "c", "b", "x", "k", "t", "r", "w", "s", "zb", "zc", "za", "f1", "f2", "f3", "-")
 OUTER = [
-    ("b", 1), ("a", 2), ("x", 1), ("c", 2), ("b", 2), ("k", 0), ("b", 3), ("x", 3), ("a", 4), ("c", 4), ("k", 1, 2), ("b", 4), ("b", 5),
-    ("x", 5), ("a", 6), ("c", 6), ("k", 3, 4), ("b", 6), ("zb", 0), ("b", 7), ("x", 7), ("k", 5, 6), ("zb", 1), ("r", 3), ("zc", 0),
-    ("za", 0), ("s", 0), ("k", 7), ("zb", 2), ("t", 0), ("t", 1), ("zc", 1), ("zc", 2), ("r", 5), ("za", 1), ("r", 7), ("za", 2), ("r", 1),
+    ("a", 2), ("b", 1), ("x", 1), ("c", 2), ("s", 0), ("b", 2), ("w", 0), ("k", 0, 1), ("x", 3), ("a", 4), ("t", 1),
+    ("t", 0), ("k", 2), ("b", 3), ("k", 3), ("a", 6), ("zb", 0), ("c", 4), ("x", 5), ("r", 1), ("b", 4), ("k", 4),
+    ("b", 5), ("zc", 0), ("x", 7), ("c", 6), ("r", 3), ("b", 6), ("k", 5, 6), ("b", 7), ("zb", 1), ("k", 7),
+    ("zb", 2), ("za", 0), ("r", 5), ("zc", 1), ("r", 7), ("zc", 2), ("za", 1), ("za", 2), ("f1", 0), ("f2", 0),
+    ("f3", 0),
 ]
 INNER = [
-    ("b", 1), ("a", 2), ("a", 4), ("x", 1), ("c", 2), ("c", 4), ("b", 2), ("b", 4), ("b", 3), ("b", 5), ("k", 0), ("x", 3), ("x", 5), ("a", 6),
-    ("k", 2, 4), ("c", 6), ("b", 6), ("b", 7), ("k", 1, 3), ("x", 7), ("k", 5, 6), ("k", 7), ("t", 0), ("t", 1), ("s", 0),
-    ("r", 3), ("r", 5), ("zb", 0), ("zc", 0), ("r", 7), ("za", 0), ("zb", 1), ("zc", 1), ("za", 1), ("r", 1), ("zb", 2), ("zc", 2), ("za", 2),
+    ("a", 2), ("a", 4), ("b", 1), ("x", 1), ("c", 4), ("c", 2), ("s", 0), ("w", 0), ("k", 0), ("a", 6), ("t", 0),
+    ("b", 4), ("k", 1, 4), ("x", 5), ("t", 1), ("b", 5), ("b", 2), ("k", 2), ("b", 3), ("x", 3), ("c", 6), ("b", 6),
+    ("k", 6), ("x", 7), ("b", 7), ("k", 5), ("r", 1), ("k", 3), ("k", 7), ("r", 5), ("r", 3), ("zb", 0), ("r", 7),
+    ("zc", 1), ("zb", 1), ("f1", 0), ("f2", 0), ("zc", 2), ("za", 1), ("zc", 0), ("zb", 2), ("za", 2), ("za", 0),
+    ("f3", 0),
 ]
-
-
-def plans_for(n):
-    return OUTER, INNER
+OUTER += [("-", 0)] * 1
+PLANS = {4: (OUTER, INNER)}
 
 
 def dense_kernel(
@@ -147,7 +150,7 @@
     ids_hbm, rw_hbm, gain_hbm, tok_hbm, gate_hbm, up_hbm, down_hbm, sg_hbm, su_hbm, sd_hbm,
     out_ref,
     ids_ref, rw_ref, gain_ref, tok, xb, xo, wtab, wr, wg, wu, wd, sg, su, sd, sh_all, sh_out,
-    pa, pb, pc, xs, xr, ys, yr, ycs, ycr, zas, zar, zbs, zbr, zcs, zcr, fs, fr, gs, gr, fin, fin_in, acc_a, acc_b, acc_c,
+    pa, pb, pc, xs, xr, ys, yr, ycs, ycr, zas, zar, zbs, zbr, zcs, zcr, fs, fr, gs, gr, fin, fin_in, last_b, last_m, acc_a, acc_b, acc_c,
     load_sem, wt_s, wt_r, we_s, we_r, sh_s, sh_r, yb_s,
     au_s, ad_s, a_r, bu_s, bd_s, b_r, cu_s, cd_s, c_r, ya_s, ya_r, yc_s, yc_r, xa_s, xa_r,
     rx_s, rx_r, ry_s, ry_r, ryc_s, ryc_r, rza_s, rza_r, rzb_s, rzb_r, rzc_s, rzc_r, f_s, f_r, g_s, g_r, o_s, o_r,
@@ -519,15 +522,10 @@
         x_copy(g).start()
 
     def do_k(code):
-        i, j = code // (n + 1), code % (n + 1)
-        both = j < n
+        i, j = code // FIELD, code % FIELD
+        both = j < FIELD - 1
         _, first = slot_group(i)
         _, second = slot_group(jnp.where(both, j, i))
-
-        @pl.when(i == 0)
-        def _():
-            for k in range(3):
-                weight_copy(k, 1 - c).wait_recv()
 
         def ready(index, g):
             @pl.when(index % 2 == 1)
@@ -546,6 +544,10 @@
             ready(j, second)
 
         compute(i, j, first, second, both)
+
+    def do_w(_):
+        for k in range(3):
+            weight_copy(k, 1 - c).wait_recv()
 
     def do_t(i):
         _, g = slot_group(i)
@@ -591,40 +593,57 @@
         zas[p] = acc_a[...].astype(jnp.bfloat16)
         send_sum(rza_copy, p, p, True)
 
-    actions = (do_a, do_c, do_b, do_x, do_k, do_t, do_r, do_s, do_zb, do_zc, do_za)
-
-    def main_step(i, carry):
-        for a, action in enumerate(actions):
-            outer, inner = (
-                sum((jnp.where(i == k, slot[a] + 1, 0) for k, slot in enumerate(plan) if slot[a] is not None), i * 0)
-                for plan in plans
-            )
-            code = jnp.where(is_end, outer, inner)
-
-            @pl.when(code > 0)
-            def _(action=action, code=code):
-                action(code - 1)
-
-        return carry
-
-    lax.fori_loop(0, max(len(plan) for plan in plans), main_step, 0)
-
     def last_copy(i):
         return remote(fs.at[i], fr.at[i], f_s.at[i], f_r.at[i], (mate_y, across, mate_x)[i])
 
     last_c = remote(gs, gr, g_s, g_r, mate_x)
 
-    sum_b(z, other_y)
-    fs[0] = acc_b[:, :tail].astype(jnp.bfloat16)
-    fs[1] = acc_b[:, tail:].astype(jnp.bfloat16)
-    last_copy(0).start()
-    last_copy(1).start()
-    sum_b(z, e)
-    fs[2] = acc_b[:, tail:].astype(jnp.bfloat16)
-    last_copy(2).start()
-    sum_c(z, e)
-    gs[...] = acc_c[:, both_keep:].astype(jnp.bfloat16)
-    last_c.start()
+    def do_f1(_):
+        sum_b(z, other_y)
+        fs[0] = acc_b[:, :tail].astype(jnp.bfloat16)
+        fs[1] = acc_b[:, tail:].astype(jnp.bfloat16)
+        last_copy(0).start()
+        last_copy(1).start()
+
+    def do_f2(_):
+        sum_b(z, e)
+        fs[2] = acc_b[:, tail:].astype(jnp.bfloat16)
+        last_copy(2).start()
+        last_b[...] = acc_b[:, :tail]
+
+    def do_f3(_):
+        sum_c(z, e)
+        gs[...] = acc_c[:, both_keep:].astype(jnp.bfloat16)
+        last_c.start()
+        last_m[...] = acc_c[:, :both_keep]
+
+    actions = (
+        (do_a, do_c, do_b, do_x, do_k, do_t, do_r, do_w),
+        (do_s, do_zb, do_zc, do_za, do_f1, do_f2, do_f3),
+    )
+
+    codes = [jnp.where(is_end, outer, inner) for outer, inner in zip(*plans)]
+
+    def main_step(i, carry):
+        code = i * 0
+        for k, value in enumerate(codes):
+            code = jnp.where(i == k, value, code)
+        kind = code // (FIELD * FIELD)
+        arg = code % (FIELD * FIELD)
+        for side_of_list, group in enumerate(actions):
+
+            @pl.when(kind // 8 == side_of_list)
+            def _(group=group):
+                for a, action in enumerate(group):
+
+                    @pl.when(kind % 8 == a)
+                    def _(action=action):
+                        action(arg)
+
+        return carry
+
+    lax.fori_loop(0, len(plans[0]), main_step, 0)
+
     sum_a(z, e)
 
     def place(low, value):
@@ -635,12 +654,12 @@
 
     place(0, acc_a[...])
     last_c.wait_recv()
-    place(keep, acc_c[:, :both_keep] + gr[...].astype(jnp.float32))
+    place(keep, last_m[...] + gr[...].astype(jnp.float32))
     for i in range(3):
         last_copy(i).wait_recv()
     place(
         middle,
-        acc_b[:, :tail] + fr[0].astype(jnp.float32) + fr[1].astype(jnp.float32) + fr[2].astype(jnp.float32),
+        last_b[...] + fr[0].astype(jnp.float32) + fr[1].astype(jnp.float32) + fr[2].astype(jnp.float32),
     )
     swap = remote(fin.at[1 - c], fin_in, o_s, o_r, mate_c)
     swap.start()
@@ -705,15 +724,12 @@
     lax.fori_loop(0, n, drain, 0)
 
 
-def slots_of(listing, n):
-    slots, last = [], len(KINDS)
-    for kind, *args in listing:
-        a = KINDS.index(kind)
-        if a <= last and (a == last or last == len(KINDS) or a < last):
-            slots.append([None] * len(KINDS))
-        slots[-1][a] = args[0] * (n + 1) + (args[1] if len(args) > 1 else n) if kind == "k" else args[0]
-        last = a
-    return slots
+def coded(plan):
+    codes = []
+    for kind, first, *second in plan:
+        arg = first * FIELD + (second[0] if second else FIELD - 1) if kind == "k" else first
+        codes.append((KINDS.index(kind) * FIELD * FIELD) + arg)
+    return codes
 
 
 def dense_exchange(
@@ -740,7 +756,7 @@
     vmem = pl.BlockSpec(memory_space=pltpu.VMEM)
     anywhere = pl.BlockSpec(memory_space=pl.ANY)
     return pl.pallas_call(
-        functools.partial(dense_kernel, n, tp_count, minor, near, wide, keep, both_keep, [slots_of(p, n) for p in plans_for(n)]),
+        functools.partial(dense_kernel, n, tp_count, minor, near, wide, keep, both_keep, [coded(plan) for plan in PLANS[n // minor]]),
         out_shape=pltpu.VMEM((rows, quarter), bf16),
         in_specs=[anywhere] * 10,
         out_specs=vmem,
@@ -782,6 +798,8 @@
             pltpu.VMEM((half, both_keep), bf16),
             pltpu.VMEM((2, half, quarter), f32),
             pltpu.VMEM((half, quarter), f32),
+            pltpu.VMEM((half, tail), f32),
+            pltpu.VMEM((half, both_keep), f32),
             pltpu.VMEM((half, keep), f32),
             pltpu.VMEM((half, 2 * tail), f32),
             pltpu.VMEM((half, 2 * both_keep), f32),

time: 59.8 us -> 51.4 us (0.86)
  Pallas kernels: 59 us -> 50.6 us
    pallas_call x1, Pallas kernels: 59 us -> 50.6 us  [dense_exchange(): pl.pallas_call(functools.partial(dense_kernel, n, tp_count, minor, near,...]
where the time goes in v3:
time: 51.4 us; the launch traced here: 51.3 us
  Pallas kernels  50.6 us (98%)
  local copies, waits for them, and re-layouts  0.66 us (1%)
    pallas_call x1, Pallas kernels, dense_exchange(): pl.pallas_call(functools.partial(dense_kernel, n, tp_count, minor, near,...  50.6 us

profile of v3, /device:TPU:0, one launch (start us, length us, event | category | flops | bytes accessed | tf_op | source)
XLA Modules:
  0.0 51.3 jit_solution(10584664173759487798)
XLA Ops:
  0.0 50.6 %dense_moe.1 = bf16[128,512]{1,0:T(8,128)(2,1)S(1)} custom-call(s32[6,128]{1,0:T(8,128)} %bitcast.10, f32[6,128]{1,0:T(8,128)} %bitcast.11, f32[1,2048]{1,0:T(1,128)} %bitcast.9, bf16[128,2048]{1,0:T(8,128)(2,1)} %tok_hbm.1, bf16[2048,256]{1,0:T(8,128)(2,1)} %bitcast.6, bf16[2048,256]{1,0:T(8,128)(2,1)} %bitcast.7, bf16[256,2048]{1,0:T(8,128)(2,1)} %bitcast.8, ...), custom_call_target="tpu_custom_call" | custom-call | tf_op jit(solution)/shard_map/dense_moe/pallas_call | solution.py:758
  50.6 0.7 %copy.12 = bf16[128,512]{1,0:T(8,128)(2,1)} copy(bf16[128,512]{1,0:T(8,128)(2,1)S(1)} %dense_moe.1) | data formatting | bytes 262144

commit v4 on v3

--- a/solution.py
+++ b/solution.py
@@ -115,10 +115,9 @@
 
 MESH = pl.DeviceIdType.MESH
 LANES = 128
-BOTH_KEEP = 3
-KEEP = 4
-WIDE = 3
-NEAR = 3
+BOTH_KEEP = 2
+WIDE = 2
+NEAR = 4
 
 
 def silu(v):
@@ -128,20 +127,17 @@
 FIELD = 16
 KINDS = ("a", "c", "b", "x", "k", "t", "r", "w", "s", "zb", "zc", "za", "f1", "f2", "f3", "-")
 OUTER = [
-    ("a", 2), ("b", 1), ("x", 1), ("c", 2), ("s", 0), ("b", 2), ("w", 0), ("k", 0, 1), ("x", 3), ("a", 4), ("t", 1),
-    ("t", 0), ("k", 2), ("b", 3), ("k", 3), ("a", 6), ("zb", 0), ("c", 4), ("x", 5), ("r", 1), ("b", 4), ("k", 4),
-    ("b", 5), ("zc", 0), ("x", 7), ("c", 6), ("r", 3), ("b", 6), ("k", 5, 6), ("b", 7), ("zb", 1), ("k", 7),
-    ("zb", 2), ("za", 0), ("r", 5), ("zc", 1), ("r", 7), ("zc", 2), ("za", 1), ("za", 2), ("f1", 0), ("f2", 0),
-    ("f3", 0),
+    ("a", 2), ("c", 2), ("b", 1), ("x", 1), ("a", 4), ("x", 3), ("w", 0), ("k", 0, 1), ("b", 3), ("a", 6), ("x", 5),
+    ("c", 4), ("b", 2), ("t", 1), ("k", 2), ("k", 3), ("b", 5), ("zb", 0), ("b", 4), ("c", 6), ("x", 7), ("k", 4, 5),
+    ("zb", 1), ("r", 3), ("s", 0), ("t", 0), ("b", 7), ("r", 1), ("zc", 1), ("b", 6), ("k", 6, 7), ("zb", 2),
+    ("r", 5), ("zc", 2), ("r", 7), ("za", 1), ("zc", 0), ("za", 2), ("f1", 0), ("za", 0), ("f2", 0), ("f3", 0),
 ]
 INNER = [
-    ("a", 2), ("a", 4), ("b", 1), ("x", 1), ("c", 4), ("c", 2), ("s", 0), ("w", 0), ("k", 0), ("a", 6), ("t", 0),
-    ("b", 4), ("k", 1, 4), ("x", 5), ("t", 1), ("b", 5), ("b", 2), ("k", 2), ("b", 3), ("x", 3), ("c", 6), ("b", 6),
-    ("k", 6), ("x", 7), ("b", 7), ("k", 5), ("r", 1), ("k", 3), ("k", 7), ("r", 5), ("r", 3), ("zb", 0), ("r", 7),
-    ("zc", 1), ("zb", 1), ("f1", 0), ("f2", 0), ("zc", 2), ("za", 1), ("zc", 0), ("zb", 2), ("za", 2), ("za", 0),
-    ("f3", 0),
+    ("a", 4), ("a", 2), ("b", 1), ("c", 2), ("a", 6), ("x", 1), ("c", 4), ("b", 3), ("b", 4), ("b", 5), ("c", 6),
+    ("x", 3), ("x", 7), ("b", 2), ("x", 5), ("b", 6), ("b", 7), ("w", 0), ("k", 1, 7), ("k", 6), ("zb", 1), ("s", 0),
+    ("k", 0, 2), ("zc", 1), ("t", 1), ("r", 7), ("k", 3, 5), ("k", 4), ("t", 0), ("zb", 0), ("zb", 2), ("zc", 2),
+    ("r", 3), ("za", 1), ("r", 5), ("zc", 0), ("r", 1), ("za", 2), ("f1", 0), ("f2", 0), ("za", 0), ("f3", 0),
 ]
-OUTER += [("-", 0)] * 1
 PLANS = {4: (OUTER, INNER)}
 
 
@@ -150,9 +146,9 @@
     ids_hbm, rw_hbm, gain_hbm, tok_hbm, gate_hbm, up_hbm, down_hbm, sg_hbm, su_hbm, sd_hbm,
     out_ref,
     ids_ref, rw_ref, gain_ref, tok, xb, xo, wtab, wr, wg, wu, wd, sg, su, sd, sh_all, sh_out,
-    pa, pb, pc, xs, xr, ys, yr, ycs, ycr, zas, zar, zbs, zbr, zcs, zcr, fs, fr, gs, gr, fin, fin_in, last_b, last_m, acc_a, acc_b, acc_c,
+    pa, pb, pc, xs, xr, ys, yr, ycs, ycr, zas, zar, zbs, zbr, zcs, zcr, fs, fr, gs, gr, head, head_in, last_b, last_m, acc_a, acc_b, acc_c,
     load_sem, wt_s, wt_r, we_s, we_r, sh_s, sh_r, yb_s,
-    au_s, ad_s, a_r, bu_s, bd_s, b_r, cu_s, cd_s, c_r, ya_s, ya_r, yc_s, yc_r, xa_s, xa_r,
+    a_s, a_r, b_s, b_r, c_s, c_r, ya_s, ya_r, yc_s, xa_s, xa_r,
     rx_s, rx_r, ry_s, ry_r, ryc_s, ryc_r, rza_s, rza_r, rzb_s, rzb_r, rzc_s, rzc_r, f_s, f_r, g_s, g_r, o_s, o_r,
 ):
     n = ep_count
@@ -173,7 +169,8 @@
     mate_x = {"tp": t2}
     mate_c = {"tp": 2 * xi + 1 - c}
     mate_y = {"ep": other_y}
-    across = {"ep": other_y, "tp": t2}
+    owner = 2 * xi + 1
+    far_owner = 2 * (1 - xi) + 1
     z_up = {"ep": lax.rem(e + minor, n)}
     z_down = {"ep": lax.rem(e + n - minor, n)}
     far = {"ep": (major - 1 - z) * minor + y}
@@ -184,7 +181,9 @@
         pl.semaphore_signal(barrier, inc=1, device_id={"ep": lax.rem(e + k, n)}, device_id_type=MESH)
     for k in range(1, tp_count):
         pl.semaphore_signal(barrier, inc=1, device_id={"tp": lax.rem(t + k, tp_count)}, device_id_type=MESH)
-    pl.semaphore_signal(barrier, inc=1, device_id=across, device_id_type=MESH)
+    for k in range(1, tp_count):
+        there = {"ep": other_y, "tp": lax.rem(t + k, tp_count)}
+        pl.semaphore_signal(barrier, inc=1, device_id=there, device_id_type=MESH)
 
     def remote(src, dst, s, r, who):
         return pltpu.make_async_remote_copy(
@@ -251,28 +250,28 @@
     for d in range(n):
         wtab[d] = weights_for(d * (tp_count // 2) + xi)
     wr[e] = weights_for(e * (tp_count // 2) + xi)
-    pl.semaphore_wait(barrier, n + tp_count - 1)
+    pl.semaphore_wait(barrier, n - 1 + 2 * (tp_count - 1))
 
     mine = pl.ds(pl.multiple_of(xi * near, LANES), near)
     theirs = pl.ds(pl.multiple_of((1 - xi) * near, LANES), near)
     shared_cols = pl.ds(2 * near, wide)
     rest = pl.ds(2 * near + wide, width - 2 * near - wide)
 
-    def line_a(g, s, who):
+    def line_a(g, who):
         ref = xb.at[g, :, mine]
-        return remote(ref, ref, s.at[g], a_r.at[g], who)
-
-    def line_b(g, s, who):
+        return remote(ref, ref, a_s, a_r.at[g // minor], who)
+
+    def line_b(g, who):
         ref = xb.at[g, :, rest]
-        return remote(ref, ref, s.at[g], b_r.at[g], who)
-
-    def line_c(g, s, who):
+        return remote(ref, ref, b_s, b_r.at[g], who)
+
+    def line_c(g, who):
         ref = xb.at[g, :, shared_cols]
-        return remote(ref, ref, s.at[g], c_r.at[g], who)
+        return remote(ref, ref, c_s, c_r.at[g // minor], who)
 
     def y_shared(g):
         ref = xb.at[g, :, shared_cols]
-        return remote(ref, ref, yc_s.at[g], yc_r.at[g], mate_y)
+        return remote(ref, ref, yc_s, xa_r.at[g], mate_y)
 
     def y_first():
         ref = xb.at[e, :, rest]
@@ -280,28 +279,36 @@
 
     def y_copy(g):
         ref = xb.at[g, :, mine]
-        return remote(ref, ref, ya_s.at[g], ya_r.at[g], mate_y)
+        return remote(ref, ref, ya_s, ya_r.at[g // minor], mate_y)
 
     def x_copy(g):
         ref = xb.at[g, :, mine]
-        return remote(ref, ref, xa_s.at[g], xa_r.at[g], mate_x)
+        return remote(ref, ref, xa_s, xa_r.at[g], mate_x)
 
     def x_arrival(g):
         ref = xb.at[g, :, theirs]
-        return remote(ref, ref, xa_s.at[g], xa_r.at[g], mate_x)
-
-    def wt_copy(k, target):
-        return remote(wtab.at[target], wr.at[e], wt_s.at[k], wt_r.at[e], {"ep": target})
-
-    def wt_arrival(g):
-        return remote(wtab.at[g], wr.at[g], wt_s.at[0], wt_r.at[g], mate_y)
+        return remote(ref, ref, xa_s, xa_r.at[g], mate_x)
+
+    def cross_arrival(g):
+        ref = xb.at[g, :, pl.ds(0, near + wide)]
+        return remote(ref, ref, xa_s, xa_r.at[g], mate_x)
+
+    def wt_copy(target):
+        return remote(wtab.at[target], wr.at[e], wt_s, wt_r, {"ep": target})
+
+    def wt_all():
+        return remote(wtab.at[pl.ds(0, n - 1)], wr.at[pl.ds(0, n - 1)], wt_s, wt_r, mate_y)
 
     def weight_copy(i, which):
         ref = (wg, wu, wd)[i].at[which]
         return remote(ref, ref, we_s.at[i], we_r.at[i], mate_c)
 
-    def sh_copy(k, slot, who):
-        return remote(sh_all.at[slot], sh_all.at[slot], sh_s.at[k], sh_r.at[k], {"tp": who})
+    def sh_copy(who):
+        return remote(sh_all.at[t], sh_all.at[t], sh_s, sh_r, {"tp": who})
+
+    def sh_rest():
+        ref = sh_all.at[pl.ds(0, tp_count - 1)]
+        return remote(ref, ref, sh_s, sh_r, mate_c)
 
     def order(j):
         k = jnp.minimum(z, major - 1 - z)
@@ -321,23 +328,23 @@
     def downs(p):
         return (p >= z) & (z > 0)
 
-    def forward(p, g, line, s_up, s_down):
+    def forward(p, g, line):
         @pl.when(ups(p))
         def _():
-            line(g, s_up, z_up).start()
+            line(g, z_up).start()
 
         @pl.when(downs(p))
         def _():
-            line(g, s_down, z_down).start()
-
-    forward(z, e, line_a, au_s, ad_s)
+            line(g, z_down).start()
+
+    for k in range(1, n):
+        wt_copy(lax.rem(e + k, n)).start()
+    forward(z, e, line_a)
     y_first().start()
-    forward(z, e, line_c, cu_s, cd_s)
+    forward(z, e, line_c)
     y_copy(e).start()
     y_shared(e).start()
-    forward(z, e, line_b, bu_s, bd_s)
-    for k in range(1, n):
-        wt_copy(k, lax.rem(e + k, n)).start()
+    forward(z, e, line_b)
     loads[2].wait()
     weight_copy(0, c).start()
     loads[3].wait()
@@ -358,25 +365,28 @@
     sh_all[t, c] = shared_in(xb[e])
     sh_all[t, 1 - c] = shared_in(xo[...])
     for k in range(1, tp_count):
-        sh_copy(k, t, lax.rem(t + k, tp_count)).start()
+        sh_copy(lax.rem(t + k, tp_count)).start()
 
     def rx_copy(g):
-        return remote(xs.at[g], xr.at[g], rx_s.at[g], rx_r.at[g], mate_x)
+        return remote(xs.at[g], xr.at[g], rx_s, rx_r.at[g], mate_x)
 
     def ry_copy(p):
-        return remote(ys.at[p], yr.at[p], ry_s.at[p], ry_r.at[p], mate_y)
+        return remote(ys.at[p], yr.at[p], ry_s, ry_r.at[p], mate_y)
 
     def ryc_copy(p):
-        return remote(ycs.at[p], ycr.at[p], ryc_s.at[p], ryc_r.at[p], mate_y)
-
-    def rzc_copy(p, lane, who):
-        return remote(zcs.at[p], zcr.at[lane, p], rzc_s.at[p], rzc_r.at[lane, p], who)
-
-    def rza_copy(p, lane, who):
-        return remote(zas.at[p], zar.at[lane, p], rza_s.at[p], rza_r.at[lane, p], who)
-
-    def rzb_copy(g, lane, who):
-        return remote(zbs.at[g], zbr.at[lane, g], rzb_s.at[g], rzb_r.at[lane, g], who)
+        return remote(ycs.at[p], ycr.at[p], ryc_s, ryc_r.at[p], mate_y)
+
+    def rzc_copy(p, slot, who):
+        return remote(zcs.at[p], zcr.at[slot], rzc_s, rzc_r.at[slot], who)
+
+    def rza_copy(p, slot, who):
+        return remote(zas.at[p], zar.at[slot], rza_s, rza_r.at[slot], who)
+
+    def rzb_copy(g, slot, who):
+        return remote(zbs.at[g], zbr.at[slot], rzb_s, rzb_r.at[slot], who)
+
+    def down_slot(key, p, to, count, extra):
+        return jnp.where(p == to, count + extra, key)
 
     diagonal = lax.broadcasted_iota(jnp.int32, (half, 2 * half), 1) == (
         lax.broadcasted_iota(jnp.int32, (half, 2 * half), 0) + c * half
@@ -435,44 +445,41 @@
         def _():
             put(1)
 
-    def add_lanes(p, acc, copy, key, received, direct):
-        below = downs(p)
-        above = ups(p)
-        if direct:
-            below &= jnp.logical_not((p == major - 1) & (z == 1))
-            above &= jnp.logical_not((p == 0) & (z == major - 2))
+    def add_lanes(p, acc, copy, key, received, extra=0, per=1):
+        count = major * per
+        below = downs(p) & jnp.logical_not((p == major - 1) & (z == 1))
+        above = ups(p) & jnp.logical_not((p == 0) & (z == major - 2))
+
+        def add(slot):
+            copy(key, slot, z_up).wait_recv()
+            acc[...] += received[slot].astype(jnp.float32)
 
         @pl.when(below)
         def _():
-            copy(key, 0, z_up).wait_recv()
-            acc[...] += received[0, key].astype(jnp.float32)
+            add(key)
 
         @pl.when(above)
         def _():
-            copy(key, 1, z_up).wait_recv()
-            acc[...] += received[1, key].astype(jnp.float32)
-
-        if direct:
-
-            @pl.when((p == z) & is_end)
-            def _():
-                copy(key, 2, far).wait_recv()
-                acc[...] += received[2, key].astype(jnp.float32)
+            add(down_slot(key, p, z, count, extra))
+
+        @pl.when((p == z) & is_end)
+        def _():
+            add(count + per + extra)
 
     def sum_b(p, g):
         acc_b[...] = pb[g]
-        add_lanes(p, acc_b, rzb_copy, g, zbr, False)
+        add_lanes(p, acc_b, rzb_copy, g, zbr, g % minor, minor)
 
     def sum_c(p, g):
         ryc_copy(p).wait_recv()
         acc_c[...] = pc[g] + ycr[p].astype(jnp.float32)
-        add_lanes(p, acc_c, rzc_copy, p, zcr, True)
+        add_lanes(p, acc_c, rzc_copy, p, zcr)
 
     def sum_a(p, g):
         rx_copy(g).wait_recv()
         ry_copy(p).wait_recv()
         acc_a[...] = pa[g] + xr[g].astype(jnp.float32) + yr[p].astype(jnp.float32)
-        add_lanes(p, acc_a, rza_copy, p, zar, True)
+        add_lanes(p, acc_a, rza_copy, p, zar)
 
     def line_order(q):
         above = major - 1 - z
@@ -480,41 +487,39 @@
         high = jnp.where(q < z, z - 1 - q, z + 1 + (q - z))
         return jnp.where(2 * z < major, low, high)
 
-    def send_sum(copy, key, p, direct):
+    def send_sum(copy, key, p, extra=0, per=1):
+        count = major * per
         whole = is_end & (p == major - 1 - z)
-        step_by = jnp.logical_not(whole) if direct else p != z
-
-        @pl.when((p > z) & step_by)
-        def _():
-            copy(key, 0, z_up).start()
-
-        @pl.when((p < z) & step_by)
-        def _():
-            copy(key, 1, z_down).start()
-
-        if direct:
-
-            @pl.when(whole)
-            def _():
-                copy(key, 2, far).start()
+
+        @pl.when((p > z) & jnp.logical_not(whole))
+        def _():
+            copy(key, key, z_up).start()
+
+        @pl.when((p < z) & jnp.logical_not(whole))
+        def _():
+            copy(key, down_slot(key, p, z - 1, count, extra), z_down).start()
+
+        @pl.when(whole)
+        def _():
+            copy(key, count + per + extra, far).start()
 
     def do_a(i):
         p, g = slot_group(i)
-        line_a(g, au_s, z_up).wait_recv()
-        forward(p, g, line_a, au_s, ad_s)
+        line_a(g, z_up).wait_recv()
+        forward(p, g, line_a)
         y_copy(g).start()
         x_copy(g).start()
 
     def do_c(i):
         p, g = slot_group(i)
-        line_c(g, cu_s, z_up).wait_recv()
-        forward(p, g, line_c, cu_s, cd_s)
+        line_c(g, z_up).wait_recv()
+        forward(p, g, line_c)
         y_shared(g).start()
 
     def do_b(i):
         p, g = slot_group(i)
-        line_b(g, bu_s, z_up).wait_recv()
-        forward(p, g, line_b, bu_s, bd_s)
+        line_b(g, z_up).wait_recv()
+        forward(p, g, line_b)
 
     def do_x(i):
         _, g = slot_group(i)
@@ -530,10 +535,11 @@
         def ready(index, g):
             @pl.when(index % 2 == 1)
             def _():
-                y_shared(g).wait_recv()
-
-            x_arrival(g).wait_recv()
-            wt_arrival(g).wait_recv()
+                cross_arrival(g).wait_recv()
+
+            @pl.when(index % 2 == 0)
+            def _():
+                x_arrival(g).wait_recv()
 
         @pl.when(i > 0)
         def _():
@@ -548,6 +554,7 @@
     def do_w(_):
         for k in range(3):
             weight_copy(k, 1 - c).wait_recv()
+        wt_all().wait_recv()
 
     def do_t(i):
         _, g = slot_group(i)
@@ -561,8 +568,7 @@
 
     def do_s(_):
         loads[8].wait()
-        for k in range(1, tp_count):
-            sh_copy(k, lax.rem(t + tp_count - k, tp_count), t).wait_recv()
+        sh_rest().wait_recv()
         share = sg.shape[1]
         for r in range(2):
             shared = jnp.zeros((half, quarter), jnp.float32)
@@ -579,24 +585,34 @@
             g = p * minor + yy
             sum_b(p, g)
             zbs[g] = acc_b[...].astype(jnp.bfloat16)
-            send_sum(rzb_copy, g, p, False)
+            send_sum(rzb_copy, g, p, g % minor, minor)
 
     def do_zc(q):
         p = line_order(q)
         sum_c(p, p * minor + y)
         zcs[p] = acc_c[...].astype(jnp.bfloat16)
-        send_sum(rzc_copy, p, p, True)
+        send_sum(rzc_copy, p, p)
 
     def do_za(q):
         p = line_order(q)
         sum_a(p, p * minor + y)
         zas[p] = acc_a[...].astype(jnp.bfloat16)
-        send_sum(rza_copy, p, p, True)
+        send_sum(rza_copy, p, p)
 
     def last_copy(i):
-        return remote(fs.at[i], fr.at[i], f_s.at[i], f_r.at[i], (mate_y, across, mate_x)[i])
-
-    last_c = remote(gs, gr, g_s, g_r, mate_x)
+        who = (
+            {"ep": other_y, "tp": owner}, {"ep": other_y, "tp": far_owner}, {"tp": far_owner}, {"tp": owner},
+        )[i]
+        return remote(fs.at[i], fr.at[c, i], f_s, f_r.at[c], who)
+
+    def last_c_copy(i):
+        return remote(gs.at[i], gr.at[c, i], g_s, g_r.at[c], ({"tp": far_owner}, {"tp": owner})[i])
+
+    def last_rows(which, count):
+        b, m = fr.at[which, pl.ds(0, count + 2)], gr.at[which, pl.ds(0, count)]
+        return remote(b, b, f_s, f_r.at[which], mate_c), remote(m, m, g_s, g_r.at[which], mate_c)
+
+    head_copy = remote(head, head_in, o_s, o_r, mate_c)
 
     def do_f1(_):
         sum_b(z, other_y)
@@ -611,117 +627,120 @@
         last_copy(2).start()
         last_b[...] = acc_b[:, :tail]
 
+        @pl.when(c == 0)
+        def _():
+            fs[3] = acc_b[:, :tail].astype(jnp.bfloat16)
+            last_copy(3).start()
+
     def do_f3(_):
         sum_c(z, e)
-        gs[...] = acc_c[:, both_keep:].astype(jnp.bfloat16)
-        last_c.start()
+        gs[0] = acc_c[:, both_keep:].astype(jnp.bfloat16)
+        last_c_copy(0).start()
         last_m[...] = acc_c[:, :both_keep]
+
+        @pl.when(c == 0)
+        def _():
+            gs[1] = acc_c[:, :both_keep].astype(jnp.bfloat16)
+            last_c_copy(1).start()
 
     actions = (
         (do_a, do_c, do_b, do_x, do_k, do_t, do_r, do_w),
         (do_s, do_zb, do_zc, do_za, do_f1, do_f2, do_f3),
     )
 
+    block = 8
     codes = [jnp.where(is_end, outer, inner) for outer, inner in zip(*plans)]
-
-    def main_step(i, carry):
-        code = i * 0
-        for k, value in enumerate(codes):
-            code = jnp.where(i == k, value, code)
-        kind = code // (FIELD * FIELD)
-        arg = code % (FIELD * FIELD)
-        for side_of_list, group in enumerate(actions):
-
-            @pl.when(kind // 8 == side_of_list)
-            def _(group=group):
-                for a, action in enumerate(group):
-
-                    @pl.when(kind % 8 == a)
-                    def _(action=action):
-                        action(arg)
-
-        return carry
-
-    lax.fori_loop(0, len(plans[0]), main_step, 0)
+    codes += [codes[-1] * 0 + FIELD * FIELD * 15] * (-len(codes) % block)
+
+    def main_block(b, carry):
+        held = codes[:block]
+        for k in range(block, len(codes), block):
+            held = [jnp.where(b == k // block, new, old) for new, old in zip(codes[k : k + block], held)]
+
+        def main_step(i, carry):
+            code = held[0]
+            for k in range(1, block):
+                code = jnp.where(i == k, held[k], code)
+            kind = code // (FIELD * FIELD)
+            arg = code % (FIELD * FIELD)
+            for part, group in enumerate(actions):
+
+                @pl.when(kind // 8 == part)
+                def _(group=group):
+                    for a, action in enumerate(group):
+
+                        @pl.when(kind % 8 == a)
+                        def _(action=action):
+                            action(arg)
+
+            return carry
+
+        return lax.fori_loop(0, block, main_step, carry)
+
+    lax.fori_loop(0, len(codes) // block, main_block, 0)
 
     sum_a(z, e)
 
-    def place(low, value):
-        for q in range(2):
-            start, stop = max(low, q * quarter), min(low + value.shape[1], (q + 1) * quarter)
-            if start < stop:
-                fin[q, :, start - q * quarter : stop - q * quarter] = value[:, start - low : stop - low]
-
-    place(0, acc_a[...])
-    last_c.wait_recv()
-    place(keep, last_m[...] + gr[...].astype(jnp.float32))
+    def total(ref):
+        return sum(ref[i].astype(jnp.float32) for i in range(1, ref.shape[0])) + ref[0].astype(jnp.float32)
+
+    @pl.when(c == 0)
+    def _():
+        out_ref[:half, :] = (acc_a[...] + sh_out[0]).astype(jnp.bfloat16)
+        head_copy.wait_recv()
+        out_ref[half:, :] = (head_in[...] + sh_out[1]).astype(jnp.bfloat16)
+        for copy in last_rows(0, 2):
+            copy.wait_send()
+
+    @pl.when(c == 1)
+    def _():
+        head[...] = acc_a[...]
+        head_copy.start()
+        for copy in last_rows(1, 1):
+            copy.wait_recv()
+        low, high = slice(0, both_keep), slice(both_keep, quarter)
+        out_ref[half:, low] = (last_m[...] + gr[1, 0].astype(jnp.float32) + sh_out[1, :, low]).astype(jnp.bfloat16)
+        out_ref[half:, high] = (last_b[...] + total(fr.at[1, pl.ds(0, 3)]) + sh_out[1, :, high]).astype(jnp.bfloat16)
+        for copy in last_rows(0, 2):
+            copy.wait_recv()
+        out_ref[:half, low] = (total(gr.at[0]) + sh_out[0, :, low]).astype(jnp.bfloat16)
+        out_ref[:half, high] = (total(fr.at[0]) + sh_out[0, :, high]).astype(jnp.bfloat16)
+        for copy in last_rows(1, 1):
+            copy.wait_send()
+        head_copy.wait_send()
+
     for i in range(3):
-        last_copy(i).wait_recv()
-    place(
-        middle,
-        last_b[...] + fr[0].astype(jnp.float32) + fr[1].astype(jnp.float32) + fr[2].astype(jnp.float32),
-    )
-    swap = remote(fin.at[1 - c], fin_in, o_s, o_r, mate_c)
-    swap.start()
-    out_ref[rows_of(c), :] = (fin[c] + sh_out[c]).astype(jnp.bfloat16)
-    swap.wait_recv()
-    out_ref[rows_of(1 - c), :] = (fin_in[...] + sh_out[1 - c]).astype(jnp.bfloat16)
-
-    swap.wait_send()
-    last_c.wait_send()
-    for i in range(3):
-        last_copy(i).wait_send()
         weight_copy(i, c).wait_send()
     y_first().wait_send()
-    for k in range(1, n):
-        wt_copy(k, lax.rem(e + k, n)).wait_send()
-    for k in range(1, tp_count):
-        sh_copy(k, t, lax.rem(t + k, tp_count)).wait_send()
-
-    def drain(i, carry):
-        p, g = slot_group(i)
-
-        def sent(line, s_up, s_down):
-            @pl.when(ups(p))
-            def _():
-                line(g, s_up, z_up).wait_send()
-
-            @pl.when(downs(p))
-            def _():
-                line(g, s_down, z_down).wait_send()
-
-        sent(line_b, bu_s, bd_s)
-
-        @pl.when(i % 2 == 0)
-        def _():
-            sent(line_a, au_s, ad_s)
-            sent(line_c, cu_s, cd_s)
-            y_copy(g).wait_send()
-            y_shared(g).wait_send()
-
-            @pl.when(p != z)
-            def _():
-                rza_copy(p, 0, z_up).wait_send()
-                rzc_copy(p, 0, z_up).wait_send()
-
-        @pl.when(i % 2 == 1)
-        def _():
-            ry_copy(p).wait_send()
-            ryc_copy(p).wait_send()
-
-        @pl.when(i > 0)
-        def _():
-            x_copy(g).wait_send()
-
-        rx_copy(g).wait_send()
-
-        @pl.when(p != z)
-        def _():
-            rzb_copy(g, 0, z_up).wait_send()
-
-        return carry
-
-    lax.fori_loop(0, n, drain, 0)
+    wt_all().wait_send()
+    sh_rest().wait_send()
+
+    def drained(ref, sem):
+        remote(ref, ref, sem, a_r.at[0], mate_c).wait_send()
+
+    def lines_sent(count):
+        groups = pl.ds(0, count)
+        drained(xb.at[groups, :, pl.ds(0, near)], a_s)
+        drained(xb.at[groups, :, pl.ds(0, wide)], c_s)
+        drained(xb.at[groups, :, pl.ds(0, 2 * (width - 2 * near - wide))], b_s)
+
+    @pl.when(is_end)
+    def _():
+        lines_sent(1)
+
+    @pl.when(jnp.logical_not(is_end))
+    def _():
+        lines_sent(major + 1)
+
+    drained(xb.at[pl.ds(0, major), :, pl.ds(0, near)], ya_s)
+    drained(xb.at[pl.ds(0, major), :, pl.ds(0, wide)], yc_s)
+    drained(xb.at[pl.ds(0, n - 1), :, pl.ds(0, near)], xa_s)
+    drained(xs, rx_s)
+    drained(ys, ry_s)
+    drained(ycs, ryc_s)
+    drained(zas.at[pl.ds(0, major - 1)], rza_s)
+    drained(zcs.at[pl.ds(0, major - 1)], rzc_s)
+    drained(zbs.at[pl.ds(0, n - minor)], rzb_s)
 
 
 def coded(plan):
@@ -746,7 +765,7 @@
     quarter = width // tp_count
     near = side * NEAR // 8 // LANES * LANES
     wide = 2 * (side * WIDE // 8 // LANES * LANES)
-    keep = side * KEEP // 8 // LANES * LANES
+    keep = quarter
     both_keep = side * BOTH_KEEP // 8 // LANES * LANES
     tail = side - keep - both_keep
     ff = expert_gate.shape[2]
@@ -787,28 +806,26 @@
             pltpu.VMEM((major, half, 2 * both_keep), bf16),
             pltpu.VMEM((major, half, 2 * both_keep), bf16),
             pltpu.VMEM((major, half, keep), bf16),
-            pltpu.VMEM((3, major, half, keep), bf16),
+            pltpu.VMEM((major + 2, half, keep), bf16),
             pltpu.VMEM((n, half, 2 * tail), bf16),
-            pltpu.VMEM((2, n, half, 2 * tail), bf16),
+            pltpu.VMEM((n + 2 * minor, half, 2 * tail), bf16),
             pltpu.VMEM((major, half, 2 * both_keep), bf16),
-            pltpu.VMEM((3, major, half, 2 * both_keep), bf16),
-            pltpu.VMEM((3, half, tail), bf16),
-            pltpu.VMEM((3, half, tail), bf16),
-            pltpu.VMEM((half, both_keep), bf16),
-            pltpu.VMEM((half, both_keep), bf16),
-            pltpu.VMEM((2, half, quarter), f32),
+            pltpu.VMEM((major + 2, half, 2 * both_keep), bf16),
+            pltpu.VMEM((4, half, tail), bf16),
+            pltpu.VMEM((2, 4, half, tail), bf16),
+            pltpu.VMEM((2, half, both_keep), bf16),
+            pltpu.VMEM((2, 2, half, both_keep), bf16),
+            pltpu.VMEM((half, quarter), f32),
             pltpu.VMEM((half, quarter), f32),
             pltpu.VMEM((half, tail), f32),
             pltpu.VMEM((half, both_keep), f32),
             pltpu.VMEM((half, keep), f32),
             pltpu.VMEM((half, 2 * tail), f32),
             pltpu.VMEM((half, 2 * both_keep), f32),
-            dma((12,)), dma((n,)), dma((n,)), dma((3,)), dma((3,)), dma((tp_count,)), dma((tp_count,)), dma,
-            dma((n,)), dma((n,)), dma((n,)), dma((n,)), dma((n,)), dma((n,)), dma((n,)), dma((n,)), dma((n,)),
-            dma((n,)), dma((n,)), dma((n,)), dma((n,)), dma((n,)), dma((n,)),
-            dma((n,)), dma((n,)), dma((major,)), dma((major,)), dma((major,)), dma((major,)),
-            dma((major,)), dma((3, major)), dma((n,)), dma((2, n)), dma((major,)), dma((3, major)),
-            dma((3,)), dma((3,)), dma, dma, dma, dma,
+            dma((12,)), dma, dma, dma((3,)), dma((3,)), dma, dma, dma,
+            dma, dma((major,)), dma, dma((n,)), dma, dma((major,)), dma, dma((major,)), dma, dma, dma((n,)),
+            dma, dma((n,)), dma, dma((major,)), dma, dma((major,)), dma, dma((major + 2,)),
+            dma, dma((n + 2 * minor,)), dma, dma((major + 2,)), dma, dma((2,)), dma, dma((2,)), dma, dma,
         ],
         compiler_params=pltpu.CompilerParams(
             collective_id=0, has_side_effects=True, vmem_limit_bytes=60 << 20

time: 51.4 us -> 44.6 us (0.87)
  Pallas kernels: 50.6 us -> 43.8 us
    pallas_call x1, Pallas kernels: 50.6 us -> 43.8 us  [dense_exchange(): pl.pallas_call(functools.partial(dense_kernel, n, tp_count, minor, near,...]
where the time goes in v4:
time: 44.6 us; the launch traced here: 44.5 us
  Pallas kernels  43.8 us (98%)
  local copies, waits for them, and re-layouts  0.66 us (1%)
    pallas_call x1, Pallas kernels, dense_exchange(): pl.pallas_call(functools.partial(dense_kernel, n, tp_count, minor, near,...  43.8 us

profile of v4, /device:TPU:0, one launch (start us, length us, event | category | flops | bytes accessed | tf_op | source)
XLA Modules:
  0.0 44.5 jit_solution(12602184636503555057)
XLA Ops:
  0.0 43.8 %dense_moe.1 = bf16[128,512]{1,0:T(8,128)(2,1)S(1)} custom-call(s32[6,128]{1,0:T(8,128)} %bitcast.10, f32[6,128]{1,0:T(8,128)} %bitcast.11, f32[1,2048]{1,0:T(1,128)} %bitcast.9, bf16[128,2048]{1,0:T(8,128)(2,1)} %tok_hbm.1, bf16[2048,256]{1,0:T(8,128)(2,1)} %bitcast.6, bf16[2048,256]{1,0:T(8,128)(2,1)} %bitcast.7, bf16[256,2048]{1,0:T(8,128)(2,1)} %bitcast.8, ...), custom_call_target="tpu_custom_call" | custom-call | tf_op jit(solution)/shard_map/dense_moe/pallas_call | solution.py:777
  43.8 0.7 %copy.12 = bf16[128,512]{1,0:T(8,128)(2,1)} copy(bf16[128,512]{1,0:T(8,128)(2,1)S(1)} %dense_moe.1) | data formatting | bytes 262144

commit v5 on v4

--- a/solution.py
+++ b/solution.py
@@ -115,7 +115,7 @@
 
 MESH = pl.DeviceIdType.MESH
 LANES = 128
-BOTH_KEEP = 2
+BOTH_KEEP = 3
 WIDE = 2
 NEAR = 4
 
@@ -126,19 +126,35 @@
 
 FIELD = 16
 KINDS = ("a", "c", "b", "x", "k", "t", "r", "w", "s", "zb", "zc", "za", "f1", "f2", "f3", "-")
-OUTER = [
-    ("a", 2), ("c", 2), ("b", 1), ("x", 1), ("a", 4), ("x", 3), ("w", 0), ("k", 0, 1), ("b", 3), ("a", 6), ("x", 5),
-    ("c", 4), ("b", 2), ("t", 1), ("k", 2), ("k", 3), ("b", 5), ("zb", 0), ("b", 4), ("c", 6), ("x", 7), ("k", 4, 5),
-    ("zb", 1), ("r", 3), ("s", 0), ("t", 0), ("b", 7), ("r", 1), ("zc", 1), ("b", 6), ("k", 6, 7), ("zb", 2),
-    ("r", 5), ("zc", 2), ("r", 7), ("za", 1), ("zc", 0), ("za", 2), ("f1", 0), ("za", 0), ("f2", 0), ("f3", 0),
+PLAN_0 = [
+    ("x", 1), ("b", 1), ("a", 2), ("x", 3), ("c", 2), ("a", 4), ("a", 6), ("b", 4), ("x", 5), ("c", 4), ("b", 2),
+    ("b", 3), ("w", 0), ("k", 3, 4), ("x", 7), ("c", 6), ("b", 5), ("k", 2, 5), ("zb", 1), ("zc", 0), ("b", 7),
+    ("k", 0, 1), ("s", 0), ("b", 6), ("k", 6, 7), ("r", 5), ("zc", 1), ("t", 1), ("zb", 2), ("zb", 0), ("zc", 2),
+    ("r", 7), ("r", 3), ("za", 1), ("t", 0), ("r", 1), ("za", 2), ("f3", 0), ("f1", 0), ("za", 0), ("f2", 0),
+    ("-", 0),
 ]
-INNER = [
-    ("a", 4), ("a", 2), ("b", 1), ("c", 2), ("a", 6), ("x", 1), ("c", 4), ("b", 3), ("b", 4), ("b", 5), ("c", 6),
-    ("x", 3), ("x", 7), ("b", 2), ("x", 5), ("b", 6), ("b", 7), ("w", 0), ("k", 1, 7), ("k", 6), ("zb", 1), ("s", 0),
-    ("k", 0, 2), ("zc", 1), ("t", 1), ("r", 7), ("k", 3, 5), ("k", 4), ("t", 0), ("zb", 0), ("zb", 2), ("zc", 2),
-    ("r", 3), ("za", 1), ("r", 5), ("zc", 0), ("r", 1), ("za", 2), ("f1", 0), ("f2", 0), ("za", 0), ("f3", 0),
+PLAN_1 = [
+    ("a", 2), ("c", 2), ("b", 1), ("a", 4), ("b", 4), ("a", 6), ("x", 3), ("c", 4), ("b", 2), ("b", 3), ("c", 6),
+    ("x", 7), ("s", 0), ("x", 5), ("b", 5), ("x", 1), ("b", 7), ("w", 0), ("k", 4, 7), ("b", 6), ("k", 0, 3),
+    ("k", 5, 6), ("r", 7), ("zc", 1), ("k", 1, 2), ("zb", 2), ("zb", 1), ("t", 1), ("r", 3), ("zb", 0), ("t", 0),
+    ("za", 1), ("zc", 2), ("r", 5), ("r", 1), ("zc", 0), ("za", 2), ("f2", 0), ("za", 0), ("f1", 0), ("f3", 0),
+    ("-", 0),
 ]
-PLANS = {4: (OUTER, INNER)}
+PLAN_2 = [
+    ("a", 4), ("a", 2), ("c", 4), ("a", 6), ("c", 2), ("c", 6), ("b", 4), ("x", 5), ("b", 5), ("b", 1), ("x", 3),
+    ("b", 3), ("b", 2), ("x", 7), ("w", 0), ("k", 4, 5), ("b", 7), ("b", 6), ("k", 6, 7), ("zb", 1), ("k", 3),
+    ("k", 0, 2), ("r", 7), ("x", 1), ("zc", 1), ("za", 1), ("r", 5), ("zc", 2), ("r", 3), ("k", 1), ("zb", 2),
+    ("zb", 0), ("s", 0), ("t", 1), ("zc", 0), ("t", 0), ("r", 1), ("za", 0), ("za", 2), ("f1", 0), ("f2", 0),
+    ("f3", 0),
+]
+PLAN_3 = [
+    ("c", 2), ("b", 1), ("x", 1), ("a", 2), ("a", 4), ("x", 3), ("c", 4), ("x", 5), ("a", 6), ("c", 6), ("x", 7),
+    ("b", 2), ("b", 5), ("b", 4), ("w", 0), ("k", 4, 5), ("zb", 1), ("b", 7), ("k", 0, 7), ("r", 5), ("b", 6),
+    ("zc", 1), ("k", 2, 6), ("zb", 2), ("r", 7), ("b", 3), ("zc", 2), ("k", 1, 3), ("t", 1), ("s", 0), ("za", 1),
+    ("za", 2), ("zb", 0), ("r", 3), ("r", 1), ("zc", 0), ("t", 0), ("za", 0), ("f1", 0), ("f2", 0), ("f3", 0),
+    ("-", 0),
+]
+PLANS = {4: (PLAN_0, PLAN_1, PLAN_2, PLAN_3)}
 
 
 def dense_kernel(
@@ -147,7 +163,7 @@
     out_ref,
     ids_ref, rw_ref, gain_ref, tok, xb, xo, wtab, wr, wg, wu, wd, sg, su, sd, sh_all, sh_out,
     pa, pb, pc, xs, xr, ys, yr, ycs, ycr, zas, zar, zbs, zbr, zcs, zcr, fs, fr, gs, gr, head, head_in, last_b, last_m, acc_a, acc_b, acc_c,
-    load_sem, wt_s, wt_r, we_s, we_r, sh_s, sh_r, yb_s,
+    line_sem, load_sem, wt_s, wt_r, we_s, we_r, sh_s, sh_r, yb_s,
     a_s, a_r, b_s, b_r, c_s, c_r, ya_s, ya_r, yc_s, xa_s, xa_r,
     rx_s, rx_r, ry_s, ry_r, ryc_s, ryc_r, rza_s, rza_r, rzb_s, rzb_r, rzc_s, rzc_r, f_s, f_r, g_s, g_r, o_s, o_r,
 ):
@@ -177,11 +193,21 @@
     is_end = (z == 0) | (z == major - 1)
 
     barrier = pltpu.get_barrier_semaphore()
-    for k in range(1, n):
-        pl.semaphore_signal(barrier, inc=1, device_id={"ep": lax.rem(e + k, n)}, device_id_type=MESH)
+
+    def greet_line(sem):
+        @pl.when(z < major - 1)
+        def _():
+            pl.semaphore_signal(sem, inc=1, device_id=z_up, device_id_type=MESH)
+
+        @pl.when(z > 0)
+        def _():
+            pl.semaphore_signal(sem, inc=1, device_id=z_down, device_id_type=MESH)
+
+    in_line = jnp.where(is_end, 1, 2)
+    greet_line(barrier)
     for k in range(1, tp_count):
         pl.semaphore_signal(barrier, inc=1, device_id={"tp": lax.rem(t + k, tp_count)}, device_id_type=MESH)
-    for k in range(1, tp_count):
+    for k in range(tp_count):
         there = {"ep": other_y, "tp": lax.rem(t + k, tp_count)}
         pl.semaphore_signal(barrier, inc=1, device_id=there, device_id_type=MESH)
 
@@ -228,7 +254,7 @@
             store(part, (v * r * gain_ref[...]).astype(jnp.bfloat16))
             return carry
 
-        lax.fori_loop(0, half // step, body, 0)
+        lax.fori_loop(0, half // step, body, 0, unroll=True)
 
     def store_own(part, value):
         xb[e, part, :] = value
@@ -250,7 +276,8 @@
     for d in range(n):
         wtab[d] = weights_for(d * (tp_count // 2) + xi)
     wr[e] = weights_for(e * (tp_count // 2) + xi)
-    pl.semaphore_wait(barrier, n - 1 + 2 * (tp_count - 1))
+    pl.semaphore_wait(barrier, 2 * tp_count - 1 + in_line)
+    greet_line(line_sem.at[0])
 
     mine = pl.ds(pl.multiple_of(xi * near, LANES), near)
     theirs = pl.ds(pl.multiple_of((1 - xi) * near, LANES), near)
@@ -337,8 +364,6 @@
         def _():
             line(g, z_down).start()
 
-    for k in range(1, n):
-        wt_copy(lax.rem(e + k, n)).start()
     forward(z, e, line_a)
     y_first().start()
     forward(z, e, line_c)
@@ -366,6 +391,12 @@
     sh_all[t, 1 - c] = shared_in(xo[...])
     for k in range(1, tp_count):
         sh_copy(lax.rem(t + k, tp_count)).start()
+    for k in range(major - 1):
+        pl.semaphore_wait(line_sem.at[k], in_line)
+        if k < major - 2:
+            greet_line(line_sem.at[k + 1])
+    for k in range(1, n):
+        wt_copy(lax.rem(e + k, n)).start()
 
     def rx_copy(g):
         return remote(xs.at[g], xr.at[g], rx_s, rx_r.at[g], mate_x)
@@ -649,7 +680,7 @@
     )
 
     block = 8
-    codes = [jnp.where(is_end, outer, inner) for outer, inner in zip(*plans)]
+    codes = [functools.reduce(lambda held, k: jnp.where(z == k, at[k], held), range(1, major), z * 0 + at[0]) for at in zip(*plans)]
     codes += [codes[-1] * 0 + FIELD * FIELD * 15] * (-len(codes) % block)
 
     def main_block(b, carry):
@@ -822,7 +853,7 @@
             pltpu.VMEM((half, keep), f32),
             pltpu.VMEM((half, 2 * tail), f32),
             pltpu.VMEM((half, 2 * both_keep), f32),
-            dma((12,)), dma, dma, dma((3,)), dma((3,)), dma, dma, dma,
+            pltpu.SemaphoreType.REGULAR((major - 1,)), dma((12,)), dma, dma, dma((3,)), dma((3,)), dma, dma, dma,
             dma, dma((major,)), dma, dma((n,)), dma, dma((major,)), dma, dma((major,)), dma, dma, dma((n,)),
             dma, dma((n,)), dma, dma((major,)), dma, dma((major,)), dma, dma((major + 2,)),
             dma, dma((n + 2 * minor,)), dma, dma((major + 2,)), dma, dma((2,)), dma, dma((2,)), dma, dma,

time: 44.6 us -> 43.4 us (0.973)
  the two profiles are of different devices: /device:TPU:0 before, /device:TPU:17 now
where the time goes in v5:
time: 43.4 us; the launch traced here: 43.3 us
  Pallas kernels  42.6 us (98%)
  local copies, waits for them, and re-layouts  0.66 us (2%)
    pallas_call x1, Pallas kernels, dense_exchange(): pl.pallas_call(functools.partial(dense_kernel, n, tp_count, minor, near,...  42.6 us

profile of v5, /device:TPU:17, one launch (start us, length us, event | category | flops | bytes accessed | tf_op | source)
XLA Modules:
  0.0 43.3 jit_solution(6815789366908940564)
XLA Ops:
  0.0 42.6 %dense_moe.1 = bf16[128,512]{1,0:T(8,128)(2,1)S(1)} custom-call(s32[6,128]{1,0:T(8,128)} %bitcast.10, f32[6,128]{1,0:T(8,128)} %bitcast.11, f32[1,2048]{1,0:T(1,128)} %bitcast.9, bf16[128,2048]{1,0:T(8,128)(2,1)} %tok_hbm.1, bf16[2048,256]{1,0:T(8,128)(2,1)} %bitcast.6, bf16[2048,256]{1,0:T(8,128)(2,1)} %bitcast.7, bf16[256,2048]{1,0:T(8,128)(2,1)} %bitcast.8, ...), custom_call_target="tpu_custom_call" | custom-call | tf_op jit(solution)/shard_map/dense_moe/pallas_call | solution.py:808
  42.6 0.7 %copy.12 = bf16[128,512]{1,0:T(8,128)(2,1)} copy(bf16[128,512]{1,0:T(8,128)(2,1)S(1)} %dense_moe.1) | data formatting | bytes 262144

commit v6 on v5

--- a/solution.py
+++ b/solution.py
@@ -115,7 +115,7 @@
 
 MESH = pl.DeviceIdType.MESH
 LANES = 128
-BOTH_KEEP = 3
+BOTH_KEEP = 2
 WIDE = 2
 NEAR = 4
 
@@ -127,31 +127,31 @@
 FIELD = 16
 KINDS = ("a", "c", "b", "x", "k", "t", "r", "w", "s", "zb", "zc", "za", "f1", "f2", "f3", "-")
 PLAN_0 = [
-    ("x", 1), ("b", 1), ("a", 2), ("x", 3), ("c", 2), ("a", 4), ("a", 6), ("b", 4), ("x", 5), ("c", 4), ("b", 2),
-    ("b", 3), ("w", 0), ("k", 3, 4), ("x", 7), ("c", 6), ("b", 5), ("k", 2, 5), ("zb", 1), ("zc", 0), ("b", 7),
-    ("k", 0, 1), ("s", 0), ("b", 6), ("k", 6, 7), ("r", 5), ("zc", 1), ("t", 1), ("zb", 2), ("zb", 0), ("zc", 2),
-    ("r", 7), ("r", 3), ("za", 1), ("t", 0), ("r", 1), ("za", 2), ("f3", 0), ("f1", 0), ("za", 0), ("f2", 0),
+    ("b", 1), ("x", 1), ("s", 0), ("b", 2), ("a", 2), ("a", 4), ("b", 3), ("c", 2), ("x", 3), ("w", 0), ("k", 2),
+    ("b", 4), ("a", 6), ("x", 5), ("c", 6), ("x", 7), ("c", 4), ("k", 1, 3), ("b", 6), ("zb", 0), ("k", 0, 6),
+    ("b", 7), ("k", 7), ("zb", 2), ("b", 5), ("k", 4, 5), ("zb", 1), ("r", 3), ("r", 5), ("zc", 1), ("zc", 2),
+    ("t", 1), ("t", 0), ("r", 7), ("zc", 0), ("f1", 0), ("za", 1), ("za", 0), ("f2", 0), ("r", 1), ("za", 2),
+    ("f3", 0),
+]
+PLAN_1 = [
+    ("a", 2), ("a", 4), ("b", 1), ("b", 3), ("x", 1), ("c", 2), ("b", 4), ("x", 3), ("a", 6), ("c", 4), ("b", 2),
+    ("c", 6), ("x", 7), ("x", 5), ("b", 6), ("b", 7), ("w", 0), ("k", 1, 6), ("b", 5), ("k", 3, 7), ("zb", 1),
+    ("k", 2, 5), ("r", 7), ("zb", 2), ("t", 1), ("zc", 1), ("k", 0), ("r", 3), ("k", 4), ("t", 0), ("zc", 2),
+    ("r", 5), ("za", 1), ("zb", 0), ("f1", 0), ("zc", 0), ("f2", 0), ("za", 2), ("r", 1), ("s", 0), ("f3", 0),
+    ("za", 0),
+]
+PLAN_2 = [
+    ("a", 2), ("a", 4), ("b", 4), ("a", 6), ("c", 4), ("x", 1), ("c", 2), ("b", 2), ("b", 3), ("x", 5), ("b", 5),
+    ("x", 7), ("c", 6), ("b", 7), ("b", 6), ("b", 1), ("x", 3), ("w", 0), ("k", 2, 6), ("k", 4, 7), ("zb", 1),
+    ("k", 3, 5), ("zc", 1), ("r", 7), ("zb", 0), ("k", 0, 1), ("t", 1), ("za", 1), ("zb", 2), ("r", 5), ("zc", 2),
+    ("t", 0), ("zc", 0), ("r", 3), ("za", 0), ("r", 1), ("za", 2), ("f1", 0), ("f2", 0), ("s", 0), ("f3", 0),
     ("-", 0),
 ]
-PLAN_1 = [
-    ("a", 2), ("c", 2), ("b", 1), ("a", 4), ("b", 4), ("a", 6), ("x", 3), ("c", 4), ("b", 2), ("b", 3), ("c", 6),
-    ("x", 7), ("s", 0), ("x", 5), ("b", 5), ("x", 1), ("b", 7), ("w", 0), ("k", 4, 7), ("b", 6), ("k", 0, 3),
-    ("k", 5, 6), ("r", 7), ("zc", 1), ("k", 1, 2), ("zb", 2), ("zb", 1), ("t", 1), ("r", 3), ("zb", 0), ("t", 0),
-    ("za", 1), ("zc", 2), ("r", 5), ("r", 1), ("zc", 0), ("za", 2), ("f2", 0), ("za", 0), ("f1", 0), ("f3", 0),
-    ("-", 0),
-]
-PLAN_2 = [
-    ("a", 4), ("a", 2), ("c", 4), ("a", 6), ("c", 2), ("c", 6), ("b", 4), ("x", 5), ("b", 5), ("b", 1), ("x", 3),
-    ("b", 3), ("b", 2), ("x", 7), ("w", 0), ("k", 4, 5), ("b", 7), ("b", 6), ("k", 6, 7), ("zb", 1), ("k", 3),
-    ("k", 0, 2), ("r", 7), ("x", 1), ("zc", 1), ("za", 1), ("r", 5), ("zc", 2), ("r", 3), ("k", 1), ("zb", 2),
-    ("zb", 0), ("s", 0), ("t", 1), ("zc", 0), ("t", 0), ("r", 1), ("za", 0), ("za", 2), ("f1", 0), ("f2", 0),
-    ("f3", 0),
-]
 PLAN_3 = [
-    ("c", 2), ("b", 1), ("x", 1), ("a", 2), ("a", 4), ("x", 3), ("c", 4), ("x", 5), ("a", 6), ("c", 6), ("x", 7),
-    ("b", 2), ("b", 5), ("b", 4), ("w", 0), ("k", 4, 5), ("zb", 1), ("b", 7), ("k", 0, 7), ("r", 5), ("b", 6),
-    ("zc", 1), ("k", 2, 6), ("zb", 2), ("r", 7), ("b", 3), ("zc", 2), ("k", 1, 3), ("t", 1), ("s", 0), ("za", 1),
-    ("za", 2), ("zb", 0), ("r", 3), ("r", 1), ("zc", 0), ("t", 0), ("za", 0), ("f1", 0), ("f2", 0), ("f3", 0),
+    ("a", 2), ("c", 2), ("b", 1), ("x", 1), ("a", 4), ("a", 6), ("b", 2), ("x", 5), ("b", 4), ("c", 4), ("w", 0),
+    ("k", 0, 4), ("b", 5), ("c", 6), ("x", 7), ("k", 1, 5), ("zb", 1), ("b", 7), ("x", 3), ("t", 1), ("b", 6),
+    ("k", 6, 7), ("b", 3), ("zb", 2), ("zc", 1), ("r", 5), ("k", 2, 3), ("zc", 2), ("r", 7), ("s", 0), ("za", 1),
+    ("zb", 0), ("za", 2), ("zc", 0), ("r", 3), ("t", 0), ("r", 1), ("f1", 0), ("f2", 0), ("za", 0), ("f3", 0),
     ("-", 0),
 ]
 PLANS = {4: (PLAN_0, PLAN_1, PLAN_2, PLAN_3)}

time: 43.4 us -> 42.6 us (0.982)
  the two profiles are of different devices: /device:TPU:17 before, /device:TPU:0 now
where the time goes in v6:
time: 42.6 us; the launch traced here: 42.5 us
  Pallas kernels  41.8 us (98%)
  local copies, waits for them, and re-layouts  0.66 us (2%)
    pallas_call x1, Pallas kernels, dense_exchange(): pl.pallas_call(functools.partial(dense_kernel, n, tp_count, minor, near,...  41.8 us

profile of v6, /device:TPU:0, one launch (start us, length us, event | category | flops | bytes accessed | tf_op | source)
XLA Modules:
  0.0 42.5 jit_solution(2724023357260116253)
XLA Ops:
  0.0 41.8 %dense_moe.1 = bf16[128,512]{1,0:T(8,128)(2,1)S(1)} custom-call(s32[6,128]{1,0:T(8,128)} %bitcast.10, f32[6,128]{1,0:T(8,128)} %bitcast.11, f32[1,2048]{1,0:T(1,128)} %bitcast.9, bf16[128,2048]{1,0:T(8,128)(2,1)} %tok_hbm.1, bf16[2048,256]{1,0:T(8,128)(2,1)} %bitcast.6, bf16[2048,256]{1,0:T(8,128)(2,1)} %bitcast.7, bf16[256,2048]{1,0:T(8,128)(2,1)} %bitcast.8, ...), custom_call_target="tpu_custom_call" | custom-call | tf_op jit(solution)/shard_map/dense_moe/pallas_call | solution.py:808
  41.8 0.7 %copy.12 = bf16[128,512]{1,0:T(8,128)(2,1)} copy(bf16[128,512]{1,0:T(8,128)(2,1)S(1)} %dense_moe.1) | data formatting | bytes 262144

commit v7 on v6

--- a/solution.py
+++ b/solution.py
@@ -164,7 +164,7 @@
     ids_ref, rw_ref, gain_ref, tok, xb, xo, wtab, wr, wg, wu, wd, sg, su, sd, sh_all, sh_out,
     pa, pb, pc, xs, xr, ys, yr, ycs, ycr, zas, zar, zbs, zbr, zcs, zcr, fs, fr, gs, gr, head, head_in, last_b, last_m, acc_a, acc_b, acc_c,
     line_sem, load_sem, wt_s, wt_r, we_s, we_r, sh_s, sh_r, yb_s,
-    a_s, a_r, b_s, b_r, c_s, c_r, ya_s, ya_r, yc_s, xa_s, xa_r,
+    a_s, a_r, b_s, b_r, c_r, ya_s, ya_r, xa_s, xa_r,
     rx_s, rx_r, ry_s, ry_r, ryc_s, ryc_r, rza_s, rza_r, rzb_s, rzb_r, rzc_s, rzc_r, f_s, f_r, g_s, g_r, o_s, o_r,
 ):
     n = ep_count
@@ -294,11 +294,11 @@
 
     def line_c(g, who):
         ref = xb.at[g, :, shared_cols]
-        return remote(ref, ref, c_s, c_r.at[g // minor], who)
+        return remote(ref, ref, a_s, c_r.at[g // minor], who)
 
     def y_shared(g):
         ref = xb.at[g, :, shared_cols]
-        return remote(ref, ref, yc_s, xa_r.at[g], mate_y)
+        return remote(ref, ref, ya_s, xa_r.at[g], mate_y)
 
     def y_first():
         ref = xb.at[e, :, rest]
@@ -710,6 +710,33 @@
 
     lax.fori_loop(0, len(codes) // block, main_block, 0)
 
+    def drained(ref, sem):
+        remote(ref, ref, sem, a_r.at[0], mate_c).wait_send()
+
+    def lines_sent(count):
+        groups = pl.ds(0, count)
+        drained(xb.at[groups, :, pl.ds(0, near + wide)], a_s)
+        drained(xb.at[groups, :, pl.ds(0, 2 * (width - 2 * near - wide))], b_s)
+
+    @pl.when(is_end)
+    def _():
+        lines_sent(1)
+
+    @pl.when(jnp.logical_not(is_end))
+    def _():
+        lines_sent(major + 1)
+
+    drained(xb.at[pl.ds(0, major), :, pl.ds(0, near + wide)], ya_s)
+    drained(xb.at[pl.ds(0, n - 1), :, pl.ds(0, near)], xa_s)
+    drained(xs, rx_s)
+    drained(ys, ry_s)
+    drained(ycs, ryc_s)
+    for i in range(3):
+        weight_copy(i, c).wait_send()
+    y_first().wait_send()
+    wt_all().wait_send()
+    sh_rest().wait_send()
+
     sum_a(z, e)
 
     def total(ref):
@@ -740,35 +767,7 @@
             copy.wait_send()
         head_copy.wait_send()
 
-    for i in range(3):
-        weight_copy(i, c).wait_send()
-    y_first().wait_send()
-    wt_all().wait_send()
-    sh_rest().wait_send()
-
-    def drained(ref, sem):
-        remote(ref, ref, sem, a_r.at[0], mate_c).wait_send()
-
-    def lines_sent(count):
-        groups = pl.ds(0, count)
-        drained(xb.at[groups, :, pl.ds(0, near)], a_s)
-        drained(xb.at[groups, :, pl.ds(0, wide)], c_s)
-        drained(xb.at[groups, :, pl.ds(0, 2 * (width - 2 * near - wide))], b_s)
-
-    @pl.when(is_end)
-    def _():
-        lines_sent(1)
-
-    @pl.when(jnp.logical_not(is_end))
-    def _():
-        lines_sent(major + 1)
-
-    drained(xb.at[pl.ds(0, major), :, pl.ds(0, near)], ya_s)
-    drained(xb.at[pl.ds(0, major), :, pl.ds(0, wide)], yc_s)
-    drained(xb.at[pl.ds(0, n - 1), :, pl.ds(0, near)], xa_s)
-    drained(xs, rx_s)
-    drained(ys, ry_s)
-    drained(ycs, ryc_s)
+
     drained(zas.at[pl.ds(0, major - 1)], rza_s)
     drained(zcs.at[pl.ds(0, major - 1)], rzc_s)
     drained(zbs.at[pl.ds(0, n - minor)], rzb_s)
@@ -854,7 +853,7 @@
             pltpu.VMEM((half, 2 * tail), f32),
             pltpu.VMEM((half, 2 * both_keep), f32),
             pltpu.SemaphoreType.REGULAR((major - 1,)), dma((12,)), dma, dma, dma((3,)), dma((3,)), dma, dma, dma,
-            dma, dma((major,)), dma, dma((n,)), dma, dma((major,)), dma, dma((major,)), dma, dma, dma((n,)),
+            dma, dma((major,)), dma, dma((n,)), dma((major,)), dma, dma((major,)), dma, dma((n,)),
             dma, dma((n,)), dma, dma((major,)), dma, dma((major,)), dma, dma((major + 2,)),
             dma, dma((n + 2 * minor,)), dma, dma((major + 2,)), dma, dma((2,)), dma, dma((2,)), dma, dma,
         ],
@@ -874,7 +873,7 @@
     pair_count = lax.axis_size("tp") // 2
     dense_bytes = 4 * ep_count * tokens.size * tokens.dtype.itemsize
     minor = 1 << (ep_count.bit_length() - 1) // 2
-    if pair_count == 2 and minor == 2 and dense_bytes <= 24 << 20:
+    if pair_count == 2 and minor == 2 and ep_count // minor in PLANS and dense_bytes <= 24 << 20:
         return dense_exchange(tokens, *rest)
     return routed_exchange(tokens, *rest)
 

time: 42.6 us -> 42.6 us (level)
  no operation moved by 1% of the time
where the time goes in v7:
time: 42.6 us; the launch traced here: 42.5 us
  Pallas kernels  41.8 us (98%)
  local copies, waits for them, and re-layouts  0.66 us (2%)
    pallas_call x1, Pallas kernels, dense_exchange(): pl.pallas_call(functools.partial(dense_kernel, n, tp_count, minor, near,...  41.8 us

profile of v7, /device:TPU:0, one launch (start us, length us, event | category | flops | bytes accessed | tf_op | source)
XLA Modules:
  0.0 42.5 jit_solution(11978910424315043270)
XLA Ops:
  0.0 41.8 %dense_moe.1 = bf16[128,512]{1,0:T(8,128)(2,1)S(1)} custom-call(s32[6,128]{1,0:T(8,128)} %bitcast.10, f32[6,128]{1,0:T(8,128)} %bitcast.11, f32[1,2048]{1,0:T(1,128)} %bitcast.9, bf16[128,2048]{1,0:T(8,128)(2,1)} %tok_hbm.1, bf16[2048,256]{1,0:T(8,128)(2,1)} %bitcast.6, bf16[2048,256]{1,0:T(8,128)(2,1)} %bitcast.7, bf16[256,2048]{1,0:T(8,128)(2,1)} %bitcast.8, ...), custom_call_target="tpu_custom_call" | custom-call | tf_op jit(solution)/shard_map/dense_moe/pallas_call | solution.py:807
  41.8 0.7 %copy.12 = bf16[128,512]{1,0:T(8,128)(2,1)} copy(bf16[128,512]{1,0:T(8,128)(2,1)S(1)} %dense_moe.1) | data formatting | bytes 262144
